TPU v7x, 32 devices: a whole 2x2x4 slice. The times are simulated.
32 devices in a mesh: ep: 16 (over z, y, x), tp: 2 (over core).
Axes of the slice: x: 2, y: 2, z: 4, core: 2. Of those that a mesh axis runs over, the one named last changes fastest.
Arguments:
- tokens: bfloat16 [4096, 2048], P('ep'), may hold values from -6 to 6
- expert_ids: int32 [4096, 4], P('ep'), may hold values from 0 to 15, all different within a row; in each aligned block of 256 rows (0 to 255, 256 to 511, ...) at most 96 rows name the same one
- gates: float32 [4096, 4], P('ep'), may hold values from 0.05 to 0.6
- cotangent: bfloat16 [4096, 2048], P('ep'), may hold values from -6 to 6
- w_gate: bfloat16 [16, 2048, 512], P('ep', None, 'tp'), may hold values from -0.125 to 0.125
- w_up: bfloat16 [16, 2048, 512], P('ep', None, 'tp'), may hold values from -0.125 to 0.125
- w_down: bfloat16 [16, 512, 2048], P('ep', 'tp'), may hold values from -0.25 to 0.25
- sh_gate: bfloat16 [2048, 512], P(None, 'tp'), may hold values from -0.125 to 0.125
- sh_up: bfloat16 [2048, 512], P(None, 'tp'), may hold values from -0.125 to 0.125
- sh_down: bfloat16 [512, 2048], P('tp'), may hold values from -0.25 to 0.25
Outputs:
- token_grad: bfloat16 [4096, 2048], P('ep', 'tp')
- gate_grad: float32 [4096, 4], P('ep')
- expert_gate_grad: float32 [16, 2048, 512], P('ep', None, 'tp')
- expert_up_grad: float32 [16, 2048, 512], P('ep', None, 'tp')
- expert_down_grad: float32 [16, 512, 2048], P('ep', 'tp')
- shared_gate_grad: float32 [2048, 512], P('ep', 'tp')
- shared_up_grad: float32 [2048, 512], P('ep', 'tp')
- shared_down_grad: float32 [512, 2048], P('tp', 'ep')
- expert_gate_rows: float32 [16, 2048], P('ep')
- expert_up_rows: float32 [16, 2048], P('ep')
- expert_down_rows: float32 [16, 512], P('ep', 'tp')
- shared_gate_rows: float32 [2048], P('ep')
- shared_up_rows: float32 [2048], P('ep')
- shared_down_rows: float32 [512], P('tp')
Inputs may be any that keep to these rules, and one draw needn't show every extreme that they name: `expert_ids`: each row names 4 different experts. Within each aligned block of 256 tokens no expert is named by more than 96 assignments, a bound that is reached in some blocks.
All inputs are finite; a program needn't handle non-finite values.
Results may differ from a plain program's by a relative error of at most 0.0085.
Values may be sent and summed in bfloat16 or wider, within the bound.
A program may use at most 128 MiB of HBM per device.

v0:
```python
import functools
import math

import jax
import jax.numpy as jnp
from jax import lax
from jax.experimental import pallas as pl
from jax.experimental.pallas import tpu as pltpu
from jax.sharding import PartitionSpec as P

BF16 = jnp.bfloat16
F32 = jnp.float32


def silu_parts(pre):
    sigmoid = jax.nn.sigmoid(pre)
    return (pre * sigmoid, sigmoid * (1.0 + pre * (1.0 - sigmoid)))


def expert_backward(inputs, cot_rows, w_g, w_u, w_d):
    gate_pre = jnp.dot(inputs, w_g, preferred_element_type=F32)
    up_pre = jnp.dot(inputs, w_u, preferred_element_type=F32)
    active, slope = silu_parts(gate_pre)
    hidden = (active * up_pre).astype(BF16)
    hidden_cot = jnp.dot(cot_rows, w_d.T, preferred_element_type=F32)
    gate_part = jnp.sum(hidden.astype(F32) * hidden_cot, axis=1)
    d_gate = (hidden_cot * up_pre * slope).astype(BF16)
    d_up = (hidden_cot * active).astype(BF16)
    contract = (((0,), (0,)), ((), ()))
    grad_g = lax.dot_general(inputs, d_gate, contract, preferred_element_type=F32)
    grad_u = lax.dot_general(inputs, d_up, contract, preferred_element_type=F32)
    grad_d = lax.dot_general(hidden, cot_rows, contract, preferred_element_type=F32)
    partial_value = jnp.dot(d_gate, w_g.T, preferred_element_type=F32) + jnp.dot(
        d_up, w_u.T, preferred_element_type=F32
    )
    return (grad_g, grad_u, grad_d, partial_value.astype(BF16), gate_part)


def plane_count(mesh):
    count = mesh.shape["ep"]
    try:
        planes = len({tuple(d.coords)[2] for d in mesh.devices.flat})
    except (AttributeError, TypeError, IndexError):
        planes = 0
    if planes < 1 or count % planes:
        planes = max(d for d in range(1, math.isqrt(count) + 1) if count % d == 0)
    return planes


def copy_to(src, dst, send, recv, ep, tp):
    return pltpu.make_async_remote_copy(
        src_ref=src,
        dst_ref=dst,
        send_sem=send,
        recv_sem=recv,
        device_id=(ep, tp),
        device_id_type=pl.DeviceIdType.MESH,
    )


def combine_kernel(
    planes, width,
    parts, sh_parts, scatter, grads,
    tok_out, grad_out,
    tp_in, sh_in, sums, plane_in, gplane_in, z_out, z_in, gz_out, gz_in, routed, gtotal,
    tp_sem, plane_sem, gplane_sem, z_sem, gz_sem,
):
    me, core = lax.axis_index("ep"), lax.axis_index("tp")
    z, q = me // width, me % width
    cols = tok_out.shape[1]
    mine = pl.ds(pl.multiple_of(core * cols, cols), cols)
    other = pl.ds(pl.multiple_of((1 - core) * cols, cols), cols)
    order = list(range(1, planes)) + [0]
    dest_z = [(z + step) % planes for step in order]
    dest_q = [(q + step) % width for step in range(width)]
    started = []

    def start(copy):
        copy.start()
        started.append(copy)
        return copy

    tp_copies = [
        start(copy_to(parts.at[dest_z[i], :, :, other], tp_in.at[i], tp_sem.at[0, i], tp_sem.at[1, i], me, 1 - core))
        for i in range(planes)
    ]
    sh_copy = start(
        copy_to(sh_parts.at[:, other], sh_in, tp_sem.at[0, planes], tp_sem.at[1, planes], me, 1 - core)
    )
    plane_copies, gplane_copies = {}, {}
    for i in range(planes):
        for d in range(1, width):
            peer = z * width + dest_q[d]
            gplane_copies[i, d] = start(
                copy_to(
                    grads.at[dest_z[i], dest_q[d]],
                    gplane_in.at[i, d - 1],
                    gplane_sem.at[0, i, d - 1],
                    gplane_sem.at[1, i, d - 1],
                    peer,
                    core,
                )
            )
        tp_copies[i].wait_recv()
        for d in range(width):
            sums[i, d] = (
                parts[dest_z[i], dest_q[d], :, mine].astype(F32) + tp_in[i, dest_q[d]].astype(F32)
            ).astype(BF16)
            if d:
                peer = z * width + dest_q[d]
                plane_copies[i, d] = start(
                    copy_to(
                        sums.at[i, d],
                        plane_in.at[i, d - 1],
                        plane_sem.at[0, i, d - 1],
                        plane_sem.at[1, i, d - 1],
                        peer,
                        core,
                    )
                )
    z_copies = []
    for i in range(planes):
        peer = dest_z[i] * width + q
        total = grads[dest_z[i], q].astype(F32)
        for d in range(1, width):
            gplane_copies[i, d].wait_recv()
            total = total + gplane_in[i, d - 1].astype(F32)
        if i < planes - 1:
            gz_out[i] = total.astype(BF16)
            z_copies.append(
                start(copy_to(gz_out.at[i], gz_in.at[i], gz_sem.at[0, i], gz_sem.at[1, i], peer, core))
            )
        else:
            gtotal[...] = total
        for d in range(1, width):
            plane_copies[i, d].wait_recv()
        acc = jnp.dot(scatter[dest_z[i], 0], sums[i, 0], preferred_element_type=F32)
        for d in range(1, width):
            acc = acc + jnp.dot(
                scatter[dest_z[i], d], plane_in[i, d - 1], preferred_element_type=F32
            )
        if i < planes - 1:
            z_out[i] = acc.astype(BF16)
            z_copies.append(
                start(copy_to(z_out.at[i], z_in.at[i], z_sem.at[0, i], z_sem.at[1, i], peer, core))
            )
        else:
            routed[...] = acc
    sh_copy.wait_recv()
    for copy in z_copies:
        copy.wait_recv()
    total = gtotal[...]
    acc = routed[...]
    for i in range(planes - 1):
        total = total + gz_in[i].astype(F32)
        acc = acc + z_in[i].astype(F32)
    grad_out[...] = total
    acc = acc + (sh_parts[:, mine].astype(F32) + sh_in[...].astype(F32))
    tok_out[...] = acc.astype(BF16)
    for copy in started:
        copy.wait_send()


def combine(planes, cols, parts, sh_parts, scatter, grads):
    width, cap = parts.shape[1:3]
    rows = sh_parts.shape[0]
    g_shape = grads.shape[2:]
    vmem = pl.BlockSpec(memory_space=pltpu.VMEM)
    far, side = max(planes - 1, 1), max(width - 1, 1)
    return pl.pallas_call(
        functools.partial(combine_kernel, planes, width),
        out_shape=(
            jax.ShapeDtypeStruct((rows, cols), BF16),
            jax.ShapeDtypeStruct(g_shape, F32),
        ),
        in_specs=[vmem] * 4,
        out_specs=(vmem, vmem),
        scratch_shapes=[
            pltpu.VMEM((planes, width, cap, cols), BF16),
            pltpu.VMEM((rows, cols), BF16),
            pltpu.VMEM((planes, width, cap, cols), BF16),
            pltpu.VMEM((planes, side, cap, cols), BF16),
            pltpu.VMEM((planes, side) + g_shape, BF16),
            pltpu.VMEM((far, rows, cols), BF16),
            pltpu.VMEM((far, rows, cols), BF16),
            pltpu.VMEM((far,) + g_shape, BF16),
            pltpu.VMEM((far,) + g_shape, BF16),
            pltpu.VMEM((rows, cols), F32),
            pltpu.VMEM(g_shape, F32),
            pltpu.SemaphoreType.DMA((2, planes + 1)),
            pltpu.SemaphoreType.DMA((2, planes, side)),
            pltpu.SemaphoreType.DMA((2, planes, side)),
            pltpu.SemaphoreType.DMA((2, far)),
            pltpu.SemaphoreType.DMA((2, far)),
        ],
        compiler_params=pltpu.CompilerParams(
            has_side_effects=True, vmem_limit_bytes=40 * 2**20
        ),
        name="combine",
    )(parts, sh_parts, scatter, grads)


def dispatch_kernel(
    planes, width, cap,
    x, table, tokens, cotangent, w_g, w_u, w_d,
    tok_out, cot_out, line_table, grads, sh_part,
    held, ready,
    table_sem, line_sem, plane_sem, own_sem, pair_sem,
):
    me, core = lax.axis_index("ep"), lax.axis_index("tp")
    z, q = me // width, me % width
    cols = x.shape[1] // 2
    mine = pl.ds(pl.multiple_of(core * cols, cols), cols)
    outs = (tok_out, cot_out)

    table_copies = []
    for step in range(1, planes):
        peer = (z + step) % planes * width + q
        copy = copy_to(
            table, line_table.at[z], table_sem.at[0, step - 1], table_sem.at[1, step - 1], peer, core
        )
        copy.start()
        table_copies.append(copy)
    line_table[z] = table[...]

    def hop(step, way):
        block = z - (step - 1) if way == 0 else z + (step - 1)
        there = z + 1 if way == 0 else z - 1
        valid = (block >= 0) & (block < planes) & (there >= 0) & (there < planes)
        block, there = jnp.clip(block, 0, planes - 1), jnp.clip(there, 0, planes - 1)
        source = x if step == 1 else held.at[block]
        copy = copy_to(
            source,
            held.at[block],
            line_sem.at[0, step - 1, way],
            line_sem.at[1, step - 1, way],
            there * width + q,
            core,
        )
        return valid, copy

    def arrival(step, way):
        block = z - step if way == 0 else z + step
        valid = (block >= 0) & (block < planes)
        block = jnp.clip(block, 0, planes - 1)
        copy = copy_to(
            held.at[block],
            held.at[block],
            line_sem.at[0, step - 1, way],
            line_sem.at[1, step - 1, way],
            me,
            1 - core,
        )
        return valid, block, copy

    def send_step(step):
        for way in range(2):
            valid, copy = hop(step, way)

            @pl.when(valid)
            def _(copy=copy):
                copy.start()

    def plane_copy(block, d, part, from_q, to_q):
        return copy_to(
            ready.at[block, d, :, pl.ds(part * cols, cols)],
            outs[part].at[block, from_q, :, mine],
            plane_sem.at[0, block, d, part],
            plane_sem.at[1, block, d, part],
            z * width + to_q,
            core,
        )

    def own_copy(block, part):
        return pltpu.make_async_copy(
            ready.at[block, 0, :, pl.ds(part * cols, cols)],
            outs[part].at[block, q, :, mine],
            own_sem.at[block, part],
        )

    def pair_copy(block, d, part):
        from_q = (q + width - d) % width
        return copy_to(
            outs[part].at[block, from_q, :, mine],
            outs[part].at[block, from_q, :, mine],
            pair_sem.at[0, block, d, part],
            pair_sem.at[1, block, d, part],
            me,
            1 - core,
        )

    def select(block, source):
        def one(index, carry):
            d = (index + 1) % width
            to_q = (q + d) % width
            expert = z * width + to_q
            ranks = line_table[block, 0, pl.ds(expert, 1), :]
            gates = line_table[block, 1, pl.ds(expert, 1), :]
            slots = lax.broadcasted_iota(jnp.int32, (cap, ranks.shape[1]), 0).astype(F32)
            hit = slots == ranks
            gate = jnp.sum(jnp.where(hit, gates, 0.0), axis=1, keepdims=True)
            rows = jnp.dot(
                jnp.where(hit, 1.0, 0.0).astype(BF16), source[...], preferred_element_type=F32
            )
            ready[block, d, :, :cols] = rows[:, :cols].astype(BF16)
            ready[block, d, :, cols:] = (rows[:, cols:] * gate).astype(BF16)

            @pl.when(d > 0)
            def _():
                for part in range(2):
                    plane_copy(block, d, part, q, to_q).start()

            @pl.when(d == 0)
            def _():
                for part in range(2):
                    own_copy(block, part).start()

            return carry

        lax.fori_loop(0, width, one, 0)

    def pass_on(block):
        for part in range(2):
            own_copy(block, part).wait()
            pair_copy(block, 0, part).start()

        def one(d, carry):
            for part in range(2):
                plane_copy(block, d, part, (q + width - d) % width, (q + d) % width).wait_recv()
                pair_copy(block, d, part).start()
            return carry

        lax.fori_loop(1, width, one, 0)

    def shared_expert():
        gate_pre = jnp.dot(tokens[...], w_g[...], preferred_element_type=F32)
        up_pre = jnp.dot(tokens[...], w_u[...], preferred_element_type=F32)
        active, slope = silu_parts(gate_pre)
        hidden = (active * up_pre).astype(BF16)
        last, first = (((1,), (1,)), ((), ())), (((0,), (0,)), ((), ()))
        hidden_cot = lax.dot_general(cotangent[...], w_d[...], last, preferred_element_type=F32)
        d_gate = (hidden_cot * up_pre * slope).astype(BF16)
        d_up = (hidden_cot * active).astype(BF16)
        part_rows = grads.shape[2] // 3
        pieces = grads.shape[3] // part_rows
        block = max(part_rows, 128)

        def one(index, carry):
            at = pl.ds(pl.multiple_of(index * block, block), block)
            rows = lax.dot_general(d_gate, w_g[at, :], last, preferred_element_type=F32)
            rows = rows + lax.dot_general(d_up, w_u[at, :], last, preferred_element_type=F32)
            sh_part[:, at] = rows.astype(BF16)
            toks = tokens[:, at]
            grad_g = lax.dot_general(toks, d_gate, first, preferred_element_type=F32).astype(BF16)
            grad_u = lax.dot_general(toks, d_up, first, preferred_element_type=F32).astype(BF16)
            grad_d = lax.dot_general(
                hidden, cotangent[:, at], first, preferred_element_type=F32
            ).astype(BF16)
            for i in range(block // part_rows):
                owner = index * (block // part_rows) + i
                oz, oq = owner // width, owner % width
                take = slice(i * part_rows, (i + 1) * part_rows)
                grads[oz, oq, :part_rows, :] = grad_g[take, :]
                grads[oz, oq, part_rows : 2 * part_rows, :] = grad_u[take, :]
                for p in range(pieces):
                    here = slice(p * part_rows, (p + 1) * part_rows)
                    grads[oz, oq, 2 * part_rows :, here] = grad_d[here, take]
            return carry

        lax.fori_loop(0, tokens.shape[1] // block, one, 0)

    send_step(1)
    select(z, x)
    shared_expert()
    for copy in table_copies:
        copy.wait_recv()
    for step in range(1, planes):
        for way in range(2):
            valid, block, copy = arrival(step, way)

            @pl.when(valid)
            def _(copy=copy):
                copy.wait_recv()

            if step < planes - 1:
                onward, hop_copy = hop(step + 1, way)

                @pl.when(onward)
                def _(hop_copy=hop_copy):
                    hop_copy.start()

            @pl.when(valid)
            def _(block=block):
                select(block, held.at[block])

        if step == 1:
            pass_on(z)
        else:
            for way in range(2):
                valid, block, copy = arrival(step - 1, way)

                @pl.when(valid)
                def _(block=block):
                    pass_on(block)

    if planes == 1:
        pass_on(z)
    else:
        for way in range(2):
            valid, block, copy = arrival(planes - 1, way)

            @pl.when(valid)
            def _(block=block):
                pass_on(block)

    for copy in table_copies:
        copy.wait_send()
    for step in range(1, planes):
        for way in range(2):
            valid, copy = hop(step, way)

            @pl.when(valid)
            def _(copy=copy):
                copy.wait_send()

    def drain(block, carry):
        def one(d, inner):
            for part in range(2):
                pair_copy(block, d, part).wait()

                @pl.when(d > 0)
                def _():
                    plane_copy(block, d, part, q, (q + d) % width).wait_send()

            return inner

        return lax.fori_loop(0, width, one, carry)

    lax.fori_loop(0, planes, drain, 0)


def dispatch(planes, x, table, cap, shared):
    experts_count, rows = table.shape[1:]
    width = experts_count // planes
    model = x.shape[1]
    vmem = pl.BlockSpec(memory_space=pltpu.VMEM)
    anywhere = pl.BlockSpec(memory_space=pl.ANY)
    landed = jax.ShapeDtypeStruct((planes, width, cap, model), BF16)
    far = max(planes - 1, 1)
    hidden_cols = shared[2].shape[1]
    deal = (planes, width, 3 * (model // experts_count), hidden_cols)
    return pl.pallas_call(
        functools.partial(dispatch_kernel, planes, width, cap),
        out_shape=(
            landed,
            landed,
            jax.ShapeDtypeStruct((planes,) + table.shape, F32),
            jax.ShapeDtypeStruct(deal, BF16),
            jax.ShapeDtypeStruct((rows, model), BF16),
        ),
        in_specs=[vmem] * 7,
        out_specs=(anywhere, anywhere, vmem, vmem, vmem),
        scratch_shapes=[
            pltpu.VMEM((planes, rows, model), BF16),
            pltpu.VMEM((planes, width, cap, model), BF16),
            pltpu.SemaphoreType.DMA((2, far)),
            pltpu.SemaphoreType.DMA((2, far, 2)),
            pltpu.SemaphoreType.DMA((2, planes, width, 2)),
            pltpu.SemaphoreType.DMA((planes, 2)),
            pltpu.SemaphoreType.DMA((2, planes, width, 2)),
        ],
        compiler_params=pltpu.CompilerParams(
            has_side_effects=True, vmem_limit_bytes=40 * 2**20
        ),
        name="dispatch",
    )(x, table, *shared)


def local(planes, tokens, expert_ids, gates, cotangent, w_gate, w_up, w_down, sh_gate, sh_up, sh_down):
    experts_count = lax.axis_size("ep")
    width = experts_count // planes
    me, core = lax.axis_index("ep"), lax.axis_index("tp")
    z, q = me // width, me % width
    tok_rows, model_width = tokens.shape
    top_count = expert_ids.shape[1]
    capacity = 3 * tok_rows * top_count // (2 * experts_count)
    half_cols = model_width // lax.axis_size("tp")
    first_col = core * half_cols

    lanes = jnp.arange(experts_count, dtype=jnp.int32)
    earlier = jnp.tril(jnp.ones((tok_rows, tok_rows), BF16), -1)

    def ranks_of(names):
        rank = jnp.dot(earlier, names.astype(BF16), preferred_element_type=F32)
        return jnp.where(names, rank.astype(jnp.int32), -1)

    mine = expert_ids[:, :, None] == lanes
    rank = ranks_of(jnp.any(mine, axis=1))
    gate_of = jnp.sum(jnp.where(mine, gates[:, :, None], 0.0), axis=1)
    slots = jnp.arange(capacity, dtype=jnp.int32)
    picked = rank.T[:, None, :] == slots[None, :, None]
    table = jnp.stack([rank.T.astype(F32), gate_of.T])
    x = jnp.concatenate(
        [
            lax.dynamic_slice_in_dim(tokens, first_col, half_cols, 1),
            lax.dynamic_slice_in_dim(cotangent, first_col, half_cols, 1),
        ],
        axis=1,
    )
    shared = (tokens, cotangent, sh_gate, sh_up, sh_down)
    got_in, got_cot, line_table, grads, shared_part = dispatch(planes, x, table, capacity, shared)
    got_in = got_in.reshape(experts_count * capacity, model_width)
    got_cot = got_cot.reshape(experts_count * capacity, model_width)
    grad_g, grad_u, grad_d, routed_part, gate_part = expert_backward(
        got_in, got_cot, w_gate[0], w_up[0], w_down[0]
    )

    part_rows = model_width // experts_count
    hidden_cols = sh_gate.shape[1]
    pieces = hidden_cols // part_rows

    senders = z * width + (q - jnp.arange(width, dtype=jnp.int32)) % width
    line_rank = line_table[:, 0][:, senders]
    scatter = (line_rank[..., None] == slots.astype(F32)).astype(BF16)

    blocks = (planes, width, capacity, model_width)
    token_grad, shared_sum = combine(
        planes, half_cols, routed_part.reshape(blocks), shared_part, scatter, grads
    )
    out_g = shared_sum[:part_rows]
    out_u = shared_sum[part_rows : 2 * part_rows]
    out_d = (
        shared_sum[2 * part_rows :]
        .reshape(part_rows, pieces, part_rows)
        .transpose(1, 0, 2)
        .reshape(hidden_cols, part_rows)
    )

    down_part = jnp.sum(out_d * out_d, axis=1)
    small = jnp.concatenate(
        [
            gate_part.reshape(experts_count, capacity),
            jnp.broadcast_to(down_part, (experts_count, hidden_cols)),
        ],
        axis=1,
    )
    small = lax.all_to_all(small, "ep", split_axis=0, concat_axis=0, tiled=True)
    back_gate, gate_norms, up_norms, shared_gate_norms, shared_up_norms = lax.psum(
        (
            small[:, :capacity],
            jnp.sum(grad_g * grad_g, axis=1),
            jnp.sum(grad_u * grad_u, axis=1),
            jnp.sum(out_g * out_g, axis=1),
            jnp.sum(out_u * out_u, axis=1),
        ),
        "tp",
    )
    down_norms = jnp.sum(small[:, capacity:], axis=0)
    token_gate = jnp.sum(jnp.where(picked, back_gate[:, :, None], 0.0), axis=1)
    gate_grad = jnp.sum(jnp.where(mine, token_gate.T[:, None, :], 0.0), axis=2) / gates
    return (
        token_grad,
        gate_grad,
        grad_g[None],
        grad_u[None],
        grad_d[None],
        out_g,
        out_u,
        out_d,
        gate_norms[None],
        up_norms[None],
        jnp.sum(grad_d * grad_d, axis=1)[None],
        shared_gate_norms,
        shared_up_norms,
        down_norms,
    )


def solution(mesh):
    placed = (
        P("ep", None),
        P("ep", None),
        P("ep", None),
        P("ep", None),
        P("ep", None, "tp"),
        P("ep", None, "tp"),
        P("ep", "tp", None),
        P(None, "tp"),
        P(None, "tp"),
        P("tp", None),
    )
    return jax.shard_map(
        functools.partial(local, plane_count(mesh)),
        mesh=mesh,
        in_specs=placed,
        out_specs=(
            P("ep", "tp"),
            P("ep", None),
            P("ep", None, "tp"),
            P("ep", None, "tp"),
            P("ep", "tp", None),
            P("ep", "tp"),
            P("ep", "tp"),
            P("tp", "ep"),
            P("ep", None),
            P("ep", None),
            P("ep", "tp"),
            P("ep"),
            P("ep"),
            P("tp"),
        ),
        check_vma=False,
    )
```

profile of v0, /device:TPU:0, one launch (start us, length us, event | category | flops | bytes accessed | tf_op | source)
XLA Modules:
  0.0 257.1 jit_solution(8347262958498721919)
XLA Ops:
  0.6 0.0 copy-start
  0.8 0.8 fusion.16
  1.5 0.2 fusion.1
  1.8 0.8 select_reduce_fusion.2
  2.5 0.0 copy-start.3
  2.6 0.0 copy-start.4
  2.6 0.0 copy-start.5
  2.6 0.0 copy-start.6
  2.6 1.4 constant_dynamic-slice_fusion
  4.0 0.1 pad_maximum_fusion.x
  4.1 0.0 copy-done.3
  4.1 0.3 copy-done.4
  4.4 0.3 copy-done.5
  4.7 0.3 copy-done.6
  5.0 1.2 copy-done.7
  6.3 105.9 %dispatch.1 = (bf16[4,4,96,2048]{3,2,1,0:T(8,128)(2,1)}, bf16[4,4,96,2048]{3,2,1,0:T(8,128)(2,1)}, f32[4,2,16,256]{3,2,1,0:T(8,128)S(1)}, bf16[4,4,384,256]{3,2,1,0:T(8,128)(2,1)S(1)}, bf16[256,2048]{1,0:T(8,128)(2,1)S(1)}) custom-call(bf16[256,2048]{1,0:T(8,128)(2,1)S(1)} %pad_maximum_fusion.x, f32[2,16,256]{2,1,0:T(8,128)S(1)} %pad_maximum_fusion.1.table, ...), custom_call_target="tpu_custom_call" | custom-call | tf_op jit(solution)/shard_map/dispatch/pallas_call | solution.py:452
  112.2 0.0 copy-start.1
  112.2 1.7 copy-done.1
  114.0 0.6 gather_fusion
  114.6 0.0 copy-done
  114.6 0.0 copy-start.8
  114.6 0.0 copy-start.14
  114.6 0.0 slice-start
  114.6 4.8 %fusion.4 = f32[1536,256]{0,1:T(8,128)S(1)} fusion(bf16[1536,2048]{1,0:T(8,128)(2,1)} %bitcast.75, bf16[1,2048,256]{2,1,0:T(8,128)(2,1)S(1)} %copy-done), kind=kOutput, calls=%fused_computation.19 | convolution fusion | flops 1610612736 | bytes 8912896 | tf_op jit(solution)/shard_map/dot_general | solution.py:21
  119.4 0.0 copy-done.8
  119.4 0.1 copy-done.14
  119.5 1.9 fusion.7
  121.4 0.0 slice-done
  121.4 0.1 slice-done.1
  121.5 0.2 copy-done.15
  121.8 3.6 %multiply_reduce_fusion.3 = (f32[1536]{0:T(1024)S(1)}, bf16[1536,256]{0,1:T(8,128)(2,1)}, bf16[1536,256]{0,1:T(8,128)(2,1)S(1)}, bf16[1536,256]{0,1:T(8,128)(2,1)}) fusion(f32[1536,256]{0,1:T(8,128)S(1)} %fusion.7, f32[1536,256]{0,1:T(8,128)S(1)} %fusion.4, bf16[1536,2048]{1,0:T(8,128)(2,1)S(1)} %bitcast.71, bf16[1,256,2048]{2,1,0:T(8,128)(2,1)S(1)} %copy-done.15), kind=kOutput, calls=%fused_computation.7 | convolution fusion | flops 1617689088 | bytes 12851200 | tf_op jit(solution)/shard_map/dot_general | solution.py:25
  125.4 0.1 reshape.114
  125.5 6.4 %fusion.2 = f32[1536,2048]{1,0:T(8,128)} fusion(bf16[1536,256]{0,1:T(8,128)(2,1)S(1)} %get-tuple-element.109, bf16[1,2048,256]{2,1,0:T(8,128)(2,1)S(1)} %copy-done), kind=kOutput, calls=%fused_computation.17 | convolution fusion | flops 1610612736 | bytes 14417920 | tf_op jit(solution)/shard_map/dot_general | solution.py:33
  131.9 0.6 compare_convert_fusion.scatter
  132.5 0.0 copy-done.9
  132.5 0.0 copy-done.10
  132.5 0.0 copy-start.2
  132.5 6.6 %add_convert_fusion = bf16[1536,2048]{1,0:T(8,128)(2,1)S(1)} fusion(f32[1536,2048]{1,0:T(8,128)} %fusion.2, bf16[1536,256]{0,1:T(8,128)(2,1)S(1)} %copy-done.10, bf16[1,2048,256]{2,1,0:T(8,128)(2,1)S(1)} %copy-done.9), kind=kOutput, calls=%fused_computation.1 | convolution fusion | flops 1616904192 | bytes 20709376 | tf_op jit(solution)/shard_map/dot_general | solution.py:33
  139.1 0.0 copy-done.2
  139.2 80.3 %combine.1 = (bf16[256,1024]{1,0:T(8,128)(2,1)S(1)}, f32[384,256]{1,0:T(8,128)S(1)}) custom-call(bf16[4,4,96,2048]{3,2,1,0:T(8,128)(2,1)S(1)} %bitcast.56, bf16[256,2048]{1,0:T(8,128)(2,1)S(1)} %get-tuple-element.23.sh_parts, bf16[4,4,256,96]{3,2,1,0:T(8,128)(2,1)S(1)} %compare_convert_fusion.scatter, bf16[4,4,384,256]{3,2,1,0:T(8,128)(2,1)S(1)} %copy-done.2), custom_call_target="tpu_custom_call" | custom-call | tf_op jit(solution)/shard_map/combine/pallas_call | solution.py:170
  219.5 0.7 multiply_reduce_fusion.4
  220.2 0.1 reshape.115
  220.3 0.2 multiply_reduce_fusion.6
  220.5 0.1 copy.53
  220.6 0.1 pad.1.clone
  220.6 0.7 all_to_all.8
  221.3 7.1 %all-to-all-start = ((f32[16,1,352]{2,1,0:T(1,128)}), f32[16,1,352]{2,1,0:T(1,128)S(1)}, u32[]{:S(2)}, u32[]{:S(2)}) async-start(f32[16,1,352]{2,1,0:T(1,128)} %all_to_all.8), calls=%async_computation | async-start | bytes 49152 | tf_op jit(solution)/shard_map/all_to_all | solution.py:547
  228.4 0.0 copy-start.11
  228.4 0.0 slice-start.2
  228.5 6.1 %multiply_reduce_fusion.2 = (f32[2048]{0:T(1024)S(1)}, f32[2048,256]{0,1:T(8,128)}) fusion(bf16[1536,256]{0,1:T(8,128)(2,1)S(1)} %get-tuple-element.109, bf16[1536,2048]{1,0:T(8,128)(2,1)} %bitcast.76), kind=kOutput, calls=%fused_computation.4 | convolution fusion | flops 1611659264 | bytes 9183232 | tf_op jit(solution)/shard_map/dot_general | solution.py:30
  234.5 0.0 copy-done.11
  234.5 6.0 %multiply_reduce_fusion.1 = (f32[2048]{0:T(1024)S(1)}, f32[2048,256]{0,1:T(8,128)}) fusion(bf16[1536,256]{0,1:T(8,128)(2,1)S(1)} %copy-done.11, bf16[1536,2048]{1,0:T(8,128)(2,1)} %bitcast.77), kind=kOutput, calls=%fused_computation.3 | convolution fusion | flops 1611659264 | bytes 9183232 | tf_op jit(solution)/shard_map/dot_general | solution.py:31
  240.6 0.0 slice-done.2
  240.6 0.0 slice-done.3
  240.6 3.7 %multiply_reduce_fusion = (f32[256]{0:T(256)}, f32[256,2048]{1,0:T(8,128)}) fusion(bf16[1536,256]{0,1:T(8,128)(2,1)S(1)} %copy-done.16, bf16[1536,2048]{1,0:T(8,128)(2,1)S(1)} %bitcast.74), kind=kOutput, calls=%fused_computation.2 | convolution fusion | flops 1611661056 | bytes 9176064 | tf_op jit(solution)/shard_map/dot_general | solution.py:32
  244.3 2.9 %copy.56 = f32[1,2048,256]{2,1,0:T(8,128)} copy(f32[1,2048,256]{1,2,0:T(8,128)} %bitcast.58) | data formatting | bytes 4194304
  247.2 2.9 %copy.55 = f32[1,2048,256]{2,1,0:T(8,128)} copy(f32[1,2048,256]{1,2,0:T(8,128)} %bitcast.57) | data formatting | bytes 4194304
  250.1 0.7 copy.54
  250.7 0.0 all-to-all-done
  250.8 0.7 slice_reduce_fusion
  251.4 4.0 %all-reduce = (f32[16,96]{1,0:T(8,128)S(1)}, f32[1,2048]{1,0:T(1,128)}, f32[1,2048]{1,0:T(1,128)}, f32[128]{0:T(128)}, f32[128]{0:T(128)}) all-reduce(f32[16,96]{1,0:T(8,128)S(1)} %slice.26, f32[1,2048]{1,0:T(1,128)S(1)} %bitcast.66, f32[1,2048]{1,0:T(1,128)S(1)} %bitcast.67, ...), channel_id=1, replica_groups=mesh['ep'=16,'tp'=2] {'tp'}, use_global_device_ids=true, to_apply=%region_4.5 | all-reduce | flops 5888 | bytes 47104 | tf_op jit(solution)/shard_map/psum | solution.py:548
  255.4 0.3 select_reduce_fusion
  255.7 0.6 div.18
  256.3 0.8 copy.61
  (27 shorter events, 0.2 us)
Async XLA Ops:
  0.6 113.9 %copy-start = (bf16[1,2048,256]{2,1,0:T(8,128)(2,1)S(1)}, bf16[1,2048,256]{2,1,0:T(8,128)(2,1)}, u32[]{:S(2)}) copy-start(bf16[1,2048,256]{2,1,0:T(8,128)(2,1)} %param.14) | copy-start | bytes 3145732
  2.5 1.6 copy-start.3
  2.6 1.8 copy-start.4
  2.6 2.2 copy-start.5
  2.6 2.5 copy-start.6
  5.0 1.2 copy-start.7
  112.2 1.8 copy-start.1
  114.6 4.8 %copy-start.8 = (bf16[1,2048,256]{2,1,0:T(8,128)(2,1)S(1)}, bf16[1,2048,256]{2,1,0:T(8,128)(2,1)}, u32[]{:S(2)}) copy-start(bf16[1,2048,256]{2,1,0:T(8,128)(2,1)} %param.15) | copy-start | bytes 3145732
  114.6 4.9 %copy-start.14 = (bf16[4,4,96,2048]{3,2,1,0:T(8,128)(2,1)S(1)}, bf16[4,4,96,2048]{3,2,1,0:T(8,128)(2,1)}, u32[]{:S(2)}) copy-start(bf16[4,4,96,2048]{3,2,1,0:T(8,128)(2,1)} %get-tuple-element.22) | copy-start | bytes 18874372
  114.6 6.8 %slice-start = ((s8[6291456]{0:T(1024)(128)(4,1)}), s8[4194304]{0:T(1024)(128)(4,1)S(1)}, s32[]{:S(2)}) async-start(s8[6291456]{0:T(1024)(128)(4,1)} %bitcast.69), calls=%async_computation.1 | async-start | bytes 8388608
  119.5 2.0 slice-start.1
  119.5 2.2 copy-start.15
  125.5 7.0 %copy-start.9 = (bf16[1,2048,256]{2,1,0:T(8,128)(2,1)S(1)}, bf16[1,2048,256]{2,1,0:T(8,128)(2,1)}, u32[]{:S(2)}) copy-start(bf16[1,2048,256]{2,1,0:T(8,128)(2,1)} %param.15) | copy-start | bytes 3145732
  125.5 7.1 %copy-start.10 = (bf16[1536,256]{0,1:T(8,128)(2,1)S(1)}, bf16[1536,256]{0,1:T(8,128)(2,1)}, u32[]{:S(2)}) copy-start(bf16[1536,256]{0,1:T(8,128)(2,1)} %get-tuple-element.110) | copy-start | bytes 2359300
  132.5 6.6 %copy-start.2 = (bf16[4,4,384,256]{3,2,1,0:T(8,128)(2,1)S(1)}, bf16[4,4,384,256]{3,2,1,0:T(8,128)(2,1)}, u32[]{:S(2)}) copy-start(bf16[4,4,384,256]{3,2,1,0:T(8,128)(2,1)} %copy-done.1) | copy-start | bytes 9437188
  221.3 29.5 %all-to-all-start = ((f32[16,1,352]{2,1,0:T(1,128)}), f32[16,1,352]{2,1,0:T(1,128)S(1)}, u32[]{:S(2)}, u32[]{:S(2)}) async-start(f32[16,1,352]{2,1,0:T(1,128)} %all_to_all.8), calls=%async_computation | async-start | bytes 49152 | tf_op jit(solution)/shard_map/all_to_all | solution.py:547
  228.4 6.1 %copy-start.11 = (bf16[1536,256]{0,1:T(8,128)(2,1)S(1)}, bf16[1536,256]{0,1:T(8,128)(2,1)}, u32[]{:S(2)}) copy-start(bf16[1536,256]{0,1:T(8,128)(2,1)} %get-tuple-element.110) | copy-start | bytes 2359300
  228.4 12.1 %slice-start.2 = ((s8[6291456]{0:T(1024)(128)(4,1)}), s8[4194304]{0:T(1024)(128)(4,1)S(1)}, s32[]{:S(2)}) async-start(s8[6291456]{0:T(1024)(128)(4,1)} %bitcast.72), calls=%async_computation.3 | async-start | bytes 8388608
  234.5 6.1 %slice-start.3 = ((s8[6291456]{0:T(1024)(128)(4,1)}), s8[2097152]{0:T(1024)(128)(4,1)S(1)}, s32[]{:S(2)}) async-start(s8[6291456]{0:T(1024)(128)(4,1)} %bitcast.72), calls=%async_computation.4 | async-start | bytes 4194304
  234.5 6.1 %copy-start.16 = (bf16[1536,256]{0,1:T(8,128)(2,1)S(1)}, bf16[1536,256]{0,1:T(8,128)(2,1)}, u32[]{:S(2)}) copy-start(bf16[1536,256]{0,1:T(8,128)(2,1)} %get-tuple-element.108) | copy-start | bytes 2359300
  247.2 8.5 %copy-start.12 = (s32[256,4]{0,1:T(4,128)S(1)}, s32[256,4]{0,1:T(4,128)}, u32[]{:S(2)}) copy-start(s32[256,4]{0,1:T(4,128)} %param.11) | copy-start | bytes 12292
  247.2 8.6 %copy-start.13 = (f32[256,4]{0,1:T(4,128)S(1)}, f32[256,4]{0,1:T(4,128)}, u32[]{:S(2)}) copy-start(f32[256,4]{0,1:T(4,128)} %param.12) | copy-start | bytes 12292
where the time goes:
time: 257 us
  Pallas kernels  186 us (72%)
  matrix products  39.3 us (15%)
  local copies, waits for them, and re-layouts  14.7 us (6%)
  starting transfers between devices  7.13 us (3%)
  other arithmetic  4.79 us (2%)
  blocking collectives  3.97 us (2%)
    pallas_call x1, Pallas kernels, dispatch(): pl.pallas_call(functools.partial(dispatch_kernel, planes, width, cap), ou...  106 us
    pallas_call x1, Pallas kernels, combine(): pl.pallas_call(functools.partial(combine_kernel, planes, width), out_shap...  80.3 us
    unnamed x46, local copies, waits for them, and re-layouts  11 us
    all_to_all x1, starting transfers between devices, local(): small = lax.all_to_all(small, 'ep', split_axis=0, concat_axis=0, tiled=True)  7.13 us
    dot_general x1, matrix products, expert_backward(): jnp.dot(d_up, w_u.T, preferred_element_type=F32)  6.6 us
    dot_general x1, matrix products, expert_backward(): jnp.dot(d_gate, w_g.T, preferred_element_type=F32)  6.43 us
    dot_general x1, matrix products, expert_backward(): lax.dot_general(inputs, d_gate, contract, preferred_element_type=F32)  6.08 us
    dot_general x1, matrix products, expert_backward(): grad_u = lax.dot_general(inputs, d_up, contract, preferred_element_type=F32)  6.05 us
  transfers between devices with their start and end apart: 1, of which 0 were waited for; matrix products, arithmetic and copies ran while one was open for 9% of the time, Pallas kernels for 0%

commit v1 on v0

v1 whole, which is shorter than its diff:
```python
import functools
import math

import jax
import jax.numpy as jnp
from jax import lax
from jax.experimental import pallas as pl
from jax.experimental.pallas import tpu as pltpu
from jax.sharding import PartitionSpec as P

BF16 = jnp.bfloat16
F32 = jnp.float32
LAST = (((1,), (1,)), ((), ()))
FIRST = (((0,), (0,)), ((), ()))


def silu_parts(pre):
    sigmoid = jax.nn.sigmoid(pre)
    return (pre * sigmoid, sigmoid * (1.0 + pre * (1.0 - sigmoid)))


def dot(left, right):
    return jnp.dot(left, right, preferred_element_type=F32)


def dot_last(left, right):
    return lax.dot_general(left, right, LAST, preferred_element_type=F32)


def dot_first(left, right):
    return lax.dot_general(left, right, FIRST, preferred_element_type=F32)


def row_sums(values):
    ones = jnp.ones((8, values.shape[1]), F32)
    sums = lax.dot_general(
        ones, values, LAST, precision=lax.Precision.HIGHEST, preferred_element_type=F32
    )
    return sums[:1]


def plane_count(mesh):
    count = mesh.shape["ep"]
    try:
        planes = len({tuple(d.coords)[2] for d in mesh.devices.flat})
    except (AttributeError, TypeError, IndexError):
        planes = 0
    if planes < 1 or count % planes:
        planes = max(d for d in range(1, math.isqrt(count) + 1) if count % d == 0)
    return planes


def copy_to(src, dst, send, recv, ep, tp):
    return pltpu.make_async_remote_copy(
        src_ref=src,
        dst_ref=dst,
        send_sem=send,
        recv_sem=recv,
        device_id=(ep, tp),
        device_id_type=pl.DeviceIdType.MESH,
    )


def layer_kernel(
    planes, width, cap,
    table, tokens, cotangent, wg_in, wu_in, wd_in, sg_in, su_in, sd_in,
    tok_out, gg_out, gu_out, gd_out, sg_out, su_out, sd_out, norm_out, down_out, sdn_out, gate_out,
    toks, cots, line_table, ready, land_t, land_c,
    w_g, w_u, w_d, s_g, s_u, s_d,
    hid, dgate, dup, tp_in, ret_in, z_out, z_in, routed,
    stage_g, stage_u, stage_d, acc_g, acc_u, acc_d,
    deal_gu, deal_d, deal_gu_in, deal_d_in, sh_part, sh_in,
    gate_part, gate_in, gate_sum, norm_part, norm_in, sdn_part,
    load_sem, table_sem, line_sem, share_sem, plane_sem, pair_sem, tp_sem, ret_sem, z_sem,
    deal_sem, misc_sem, gate_sem, sdn_sem, stage_sem,
):
    me, core = lax.axis_index("ep"), lax.axis_index("tp")
    z, q = me // width, me % width
    experts = planes * width
    rows, model = tokens.shape
    cols = model // 2
    hidden = w_g.shape[1]
    slots = width * cap
    take = model // experts
    span = width * take
    mine = pl.ds(pl.multiple_of(core * cols, cols), cols)
    other = pl.ds(pl.multiple_of((1 - core) * cols, cols), cols)
    parts = (toks, cots)
    lands = (land_t, land_c)

    def landed(ref, sem):
        copy_to(ref, ref, sem, sem, me, 1 - core).wait_recv()

    def sent(ref, sem):
        copy_to(ref, ref, sem, sem, me, 1 - core).wait_send()

    loads = [
        pltpu.make_async_copy(src, dst, load_sem.at[i])
        for i, (src, dst) in enumerate(
            (
                (tokens, toks.at[z]),
                (cotangent, cots.at[z]),
                (sg_in, s_g),
                (su_in, s_u),
                (sd_in, s_d),
                (wg_in, w_g),
                (wu_in, w_u),
                (wd_in, w_d),
            )
        )
    ]
    for load in loads:
        load.start()

    def table_copy(step):
        peer = (z + step) % planes * width + q
        return copy_to(
            table, line_table.at[z], table_sem.at[0, step - 1], table_sem.at[1, step - 1], peer, core
        )

    for step in range(1, planes):
        table_copy(step).start()
    line_table[z] = table[...]

    def line_copy(way, block, part):
        there = jnp.clip(z + 1 - 2 * way, 0, planes - 1)
        ref = parts[part].at[block, :, mine]
        return copy_to(
            ref, ref, line_sem.at[0, way, block, part], line_sem.at[1, way, block, part],
            there * width + q, core,
        )

    def onward(way):
        there = z + 1 - 2 * way
        return (there >= 0) & (there < planes)

    def share_copy(block, part):
        ref = parts[part].at[block, :, mine]
        return copy_to(ref, ref, share_sem.at[0, block, part], share_sem.at[1, block, part], me, 1 - core)

    def plane_copy(block, d, part):
        to_q = (q + d) % width
        return copy_to(
            ready.at[block, part, to_q],
            lands[part].at[block, q, :, mine],
            plane_sem.at[0, block, d, part],
            plane_sem.at[1, block, d, part],
            z * width + to_q,
            core,
        )

    def pair_copy(block, d, part):
        ref = lands[part].at[block, (q + width - d) % width, :, mine]
        return copy_to(
            ref, ref, pair_sem.at[0, block, d, part], pair_sem.at[1, block, d, part], me, 1 - core
        )

    def tp_copy(block):
        return copy_to(
            ready.at[block, 1 - core], tp_in.at[block], tp_sem.at[0, block], tp_sem.at[1, block],
            me, 1 - core,
        )

    def ret_copy(block, d):
        to_q = (q + d) % width
        return copy_to(
            tp_in.at[block, to_q], ret_in.at[block, q], ret_sem.at[0, block, d], ret_sem.at[1, block, d],
            z * width + to_q, core,
        )

    def z_copy(block):
        return copy_to(
            z_out.at[block], z_in.at[z], z_sem.at[0, block], z_sem.at[1, z], block * width + q, core
        )

    def hits(block):
        ranks = line_table[block, 0, z]
        at = lax.broadcasted_iota(jnp.int32, (width, cap, rows), 1).astype(F32)
        return (at == ranks).reshape(slots, rows)

    def each(step, act):
        def one(way, carry):
            block = z - step + 2 * step * way
            valid = (step >= 0) & (block >= 0) & (block < planes) & ((step > 0) | (way == 0))

            @pl.when(valid)
            def _():
                act(jnp.clip(block, 0, planes - 1), way)

            return carry

        lax.fori_loop(0, 2, one, 0)

    def select(part, block):
        hit = hits(block)
        picked = dot(jnp.where(hit, 1.0, 0.0).astype(BF16), parts[part][block, :, mine])
        if part == 1:
            gates = line_table[block, 1, z]
            gates = jnp.broadcast_to(gates, (width, cap, rows)).reshape(slots, rows)
            picked = picked * jnp.sum(jnp.where(hit, gates, 0.0), axis=1, keepdims=True)
        ready[block, part] = picked.astype(BF16).reshape(width, cap, cols)

        def one(d, carry):
            plane_copy(block, d, part).start()
            return carry

        lax.fori_loop(1, width, one, 0)
        lands[part][block, q, :, mine] = ready[block, part, q]
        pair_copy(block, 0, part).start()

    def pass_on(block, way):
        for part in range(2):

            def one(d, carry):
                landed(lands[part].at[block, q, :, mine], plane_sem.at[1, block, d, part])
                pair_copy(block, d, part).start()
                return carry

            lax.fori_loop(1, width, one, 0)

    def shared(block, way):
        for part in range(2):

            @pl.when(block != z)
            def _():
                landed(parts[part].at[block, :, other], share_sem.at[1, block, part])

        gate_pre = dot(toks[block], s_g[...])
        up_pre = dot(toks[block], s_u[...])
        active, slope = silu_parts(gate_pre)
        h = (active * up_pre).astype(BF16)
        h_cot = dot_last(cots[block], s_d[...])
        d_gate = (h_cot * up_pre * slope).astype(BF16)
        d_up = (h_cot * active).astype(BF16)
        here = pl.ds(pl.multiple_of(z * span, span), span)
        acc_g[...] += dot_first(toks[block, :, here], d_gate)
        acc_u[...] += dot_first(toks[block, :, here], d_up)
        acc_d[...] += dot_first(h, cots[block, :, here])

        @pl.when(block == z)
        def _():
            wide = cols // 2

            def one(i, carry):
                at = pl.ds(pl.multiple_of(i * wide, wide), wide)
                sh_part[:, at] = (dot_last(d_gate, s_g[at, :]) + dot_last(d_up, s_u[at, :])).astype(BF16)
                return carry

            lax.fori_loop(0, model // wide, one, 0)
            sh_copy.start()

    sh_copy = copy_to(sh_part.at[:, other], sh_in, misc_sem.at[0, 0], misc_sem.at[1, 0], me, 1 - core)

    def compute(block, way):
        for part in range(2):

            def one(d, carry):
                ref = lands[part].at[block, (q + width - d) % width, :, other]
                landed(ref, pair_sem.at[1, block, d, part])
                return carry

            lax.fori_loop(0, width, one, 0)

            def freed(d, carry):
                sent(ready.at[block, part, 0], plane_sem.at[0, block, d, part])
                return carry

            lax.fori_loop(1, width, freed, 0)
        inputs = land_t[block].reshape(slots, model)
        gate_pre = dot(inputs, w_g[...])
        up_pre = dot(inputs, w_u[...])
        active, slope = silu_parts(gate_pre)
        h = (active * up_pre).astype(BF16)
        h_cot = dot_last(land_c[block].reshape(slots, model), w_d[...])
        d_gate = (h_cot * up_pre * slope).astype(BF16)
        d_up = (h_cot * active).astype(BF16)
        hid[block] = h
        dgate[block] = d_gate
        dup[block] = d_up
        wide = cols // 2

        def half(which):
            def one(i, carry):
                at = pl.ds(pl.multiple_of(which * cols + i * wide, wide), wide)
                out = dot_last(d_gate, w_g[at, :]) + dot_last(d_up, w_u[at, :])
                here = pl.ds(pl.multiple_of(i * wide, wide), wide)
                ready[block, which, :, :, here] = out.astype(BF16).reshape(width, cap, wide)
                return carry

            lax.fori_loop(0, 2, one, 0)

        def one(i, carry):
            half((1 - core) * (1 - i) + core * i)

            @pl.when(i == 0)
            def _():
                tp_copy(block).start()

            return carry

        lax.fori_loop(0, 2, one, 0)
        gate_part[block] = row_sums(h.astype(F32) * h_cot)

    def sums(block, way):
        landed(tp_in.at[block], tp_sem.at[1, block])
        tp_in[block] = (ready[block, core].astype(F32) + tp_in[block].astype(F32)).astype(BF16)

        def one(d, carry):
            ret_copy(block, d).start()
            return carry

        lax.fori_loop(1, width, one, 0)
        ret_in[block, q] = tp_in[block, q]

    def scatter(block, way):
        def one(d, carry):
            landed(ret_in.at[block, q], ret_sem.at[1, block, d])
            return carry

        lax.fori_loop(1, width, one, 0)
        hit = jnp.where(hits(block), 1.0, 0.0).astype(BF16)
        back = dot_first(hit, ret_in[block].reshape(slots, cols))

        @pl.when(block == z)
        def _():
            routed[...] = back

        @pl.when(block != z)
        def _():
            z_out[block] = back.astype(BF16)
            z_copy(block).start()

    for part in range(2):
        loads[part].wait()
        for way in range(2):

            @pl.when(onward(way))
            def _():
                line_copy(way, z, part).start()

    acc_g[...] = jnp.zeros_like(acc_g)
    acc_u[...] = jnp.zeros_like(acc_u)
    acc_d[...] = jnp.zeros_like(acc_d)

    def body(step, carry):
        @pl.when(step == 1)
        def _():
            for load in loads[2:]:
                load.wait()
            for other_step in range(1, planes):
                landed(line_table.at[z], table_sem.at[1, other_step - 1])

        for part in range(2):

            def arrive(block, way):
                @pl.when(step > 0)
                def _():
                    landed(parts[part].at[block, :, mine], line_sem.at[1, way, block, part])

                    @pl.when(onward(way))
                    def _():
                        line_copy(way, block, part).start()

                    share_copy(block, part).start()

            each(step, arrive)
            each(step, lambda block, way: select(part, block))
        each(step - 1, shared)
        each(step - 1, pass_on)
        each(step - 1, compute)
        each(step - 1, sums)
        each(step - 2, scatter)
        return carry

    lax.fori_loop(0, planes + 1, body, 0)

    for p in range(width):
        at = slice(p * take, (p + 1) * take)
        deal_gu[p, 0] = acc_g[at, :].astype(BF16)
        deal_gu[p, 1] = acc_u[at, :].astype(BF16)
        deal_d[p] = acc_d[:, at].astype(BF16)

    def deal_copies(d):
        to_q = (q + d) % width
        peer = z * width + to_q
        return (
            copy_to(deal_gu.at[to_q], deal_gu_in.at[d], deal_sem.at[0, d, 0], deal_sem.at[1, d, 0], peer, core),
            copy_to(deal_d.at[to_q], deal_d_in.at[d], deal_sem.at[0, d, 1], deal_sem.at[1, d, 1], peer, core),
        )

    def deal(d, carry):
        for copy in deal_copies(d):
            copy.start()
        return carry

    lax.fori_loop(1, width, deal, 0)
    gate_pair = copy_to(gate_part, gate_in, misc_sem.at[0, 1], misc_sem.at[1, 1], me, 1 - core)
    gate_pair.start()
    gate_pair.wait_recv()
    gate_sum[...] = gate_part[...] + gate_in[...]
    gate_out[me] = gate_sum[z]

    def gate_copy(step):
        peer = (me + step) % experts
        return copy_to(
            gate_sum.at[peer // width], gate_out.at[me], gate_sem.at[0, step], gate_sem.at[1, step], peer, core
        )

    def send_gate(step, carry):
        gate_copy(step).start()
        return carry

    lax.fori_loop(1, experts, send_gate, 0)

    wide = stage_g.shape[1]
    chunks = model // wide

    def stage_copies(i, slot):
        at = pl.ds(pl.multiple_of(i * wide, wide), wide)
        return (
            pltpu.make_async_copy(stage_g.at[slot], gg_out.at[at, :], stage_sem.at[slot, 0]),
            pltpu.make_async_copy(stage_u.at[slot], gu_out.at[at, :], stage_sem.at[slot, 1]),
            pltpu.make_async_copy(stage_d.at[slot], gd_out.at[:, at], stage_sem.at[slot, 2]),
        )

    down_out[...] = jnp.zeros_like(down_out)
    norm_part[...] = jnp.zeros_like(norm_part)

    def weight_grads(i, carry):
        slot = i % 2
        at = pl.ds(pl.multiple_of(i * wide, wide), wide)

        @pl.when(i >= 2)
        def _():
            for copy in stage_copies(i - 2, slot):
                copy.wait()

        block_rows = land_t[:, :, :, at].reshape(planes * slots, wide)
        grad = dot_first(block_rows, dgate[...].reshape(planes * slots, hidden))
        stage_g[slot] = grad
        norm_part[0:1, at] = row_sums(grad * grad)
        grad = dot_first(block_rows, dup[...].reshape(planes * slots, hidden))
        stage_u[slot] = grad
        norm_part[1:2, at] = row_sums(grad * grad)
        block_rows = land_c[:, :, :, at].reshape(planes * slots, wide)
        grad = dot_first(hid[...].reshape(planes * slots, hidden), block_rows)
        stage_d[slot] = grad
        down_out[...] += row_sums(grad * grad)
        for copy in stage_copies(i, slot):
            copy.start()
        return carry

    lax.fori_loop(0, chunks, weight_grads, 0)
    each(planes - 1, scatter)

    def deal_done(d, carry):
        for copy in deal_copies(d):
            copy.wait_recv()
        return carry

    lax.fori_loop(1, width, deal_done, 0)
    grad_g, grad_u, grad_d = deal_gu[q, 0].astype(F32), deal_gu[q, 1].astype(F32), deal_d[q].astype(F32)
    for d in range(1, width):
        grad_g = grad_g + deal_gu_in[d, 0].astype(F32)
        grad_u = grad_u + deal_gu_in[d, 1].astype(F32)
        grad_d = grad_d + deal_d_in[d].astype(F32)
    sg_out[...] = grad_g
    su_out[...] = grad_u
    sd_out[...] = grad_d
    norm_part[2:3, :take] = row_sums(grad_g * grad_g)
    norm_part[3:4, :take] = row_sums(grad_u * grad_u)
    norm_pair = copy_to(norm_part, norm_in, misc_sem.at[0, 2], misc_sem.at[1, 2], me, 1 - core)
    norm_pair.start()
    sdn_part[...] = row_sums(grad_d * grad_d)
    sdn_out[me] = sdn_part[...]

    def sdn_copy(step):
        return copy_to(
            sdn_part, sdn_out.at[me], sdn_sem.at[0, step], sdn_sem.at[1, step], (me + step) % experts, core
        )

    def send_sdn(step, carry):
        sdn_copy(step).start()
        return carry

    lax.fori_loop(1, experts, send_sdn, 0)
    sh_copy.wait_recv()
    total = routed[...] + (sh_part[:, mine].astype(F32) + sh_in[...].astype(F32))
    routed[...] = total
    norm_pair.wait_recv()
    norm_out[...] = norm_part[...] + norm_in[...]

    def gather(step, carry):
        source = (z + step) % planes
        landed(z_in.at[source], z_sem.at[1, source])
        routed[...] += z_in[source].astype(F32)
        return carry

    lax.fori_loop(1, planes, gather, 0)
    tok_out[...] = routed[...].astype(BF16)

    def small_done(step, carry):
        gate_copy(step).wait()
        sdn_copy(step).wait()
        return carry

    lax.fori_loop(1, experts, small_done, 0)
    for i in range(max(chunks - 2, 0), chunks):
        for copy in stage_copies(i, i % 2):
            copy.wait()
    for step in range(1, planes):
        table_copy(step).wait_send()
    sh_copy.wait_send()
    gate_pair.wait_send()
    norm_pair.wait_send()

    def deal_sent(d, carry):
        for copy in deal_copies(d):
            copy.wait_send()
        return carry

    lax.fori_loop(1, width, deal_sent, 0)

    def drain(block, carry):
        for part in range(2):
            for way in range(2):
                behind = (block <= z) if way == 0 else (block >= z)

                @pl.when(behind & onward(way))
                def _():
                    line_copy(way, block, part).wait_send()

            @pl.when(block != z)
            def _():
                share_copy(block, part).wait_send()

            def pairs(d, inner):
                pair_copy(block, d, part).wait_send()
                return inner

            lax.fori_loop(0, width, pairs, 0)
        tp_copy(block).wait_send()

        def returns(d, inner):
            ret_copy(block, d).wait_send()
            return inner

        lax.fori_loop(1, width, returns, 0)

        @pl.when(block != z)
        def _():
            z_copy(block).wait_send()

        return carry

    lax.fori_loop(0, planes, drain, 0)


def layer(planes, cap, table, tokens, cotangent, w_gate, w_up, w_down, sh_gate, sh_up, sh_down):
    width = table.shape[2]
    experts = planes * width
    rows, model = tokens.shape
    cols, hidden = model // 2, w_gate.shape[1]
    take = model // experts
    span = width * take
    slots = width * cap
    wide = min(256, model)
    vmem = pl.BlockSpec(memory_space=pltpu.VMEM)
    hbm = pl.BlockSpec(memory_space=pltpu.HBM)
    out = jax.ShapeDtypeStruct
    dma = pltpu.SemaphoreType.DMA
    far = max(planes - 1, 1)
    return pl.pallas_call(
        functools.partial(layer_kernel, planes, width, cap),
        out_shape=(
            out((rows, cols), BF16),
            out((model, hidden), F32),
            out((model, hidden), F32),
            out((hidden, model), F32),
            out((take, hidden), F32),
            out((take, hidden), F32),
            out((hidden, take), F32),
            out((8, model), F32),
            out((1, hidden), F32),
            out((experts, 1, hidden), F32),
            out((experts, 1, slots), F32),
        ),
        in_specs=[vmem] + [hbm] * 8,
        out_specs=(vmem, hbm, hbm, hbm) + (vmem,) * 7,
        scratch_shapes=[
            pltpu.VMEM((planes, rows, model), BF16),
            pltpu.VMEM((planes, rows, model), BF16),
            pltpu.VMEM((planes,) + table.shape, F32),
            pltpu.VMEM((planes, 2, width, cap, cols), BF16),
            pltpu.VMEM((planes, width, cap, model), BF16),
            pltpu.VMEM((planes, width, cap, model), BF16),
            pltpu.VMEM((model, hidden), BF16),
            pltpu.VMEM((model, hidden), BF16),
            pltpu.VMEM((hidden, model), BF16),
            pltpu.VMEM((model, hidden), BF16),
            pltpu.VMEM((model, hidden), BF16),
            pltpu.VMEM((hidden, model), BF16),
            pltpu.VMEM((planes, slots, hidden), BF16),
            pltpu.VMEM((planes, slots, hidden), BF16),
            pltpu.VMEM((planes, slots, hidden), BF16),
            pltpu.VMEM((planes, width, cap, cols), BF16),
            pltpu.VMEM((planes, width, cap, cols), BF16),
            pltpu.VMEM((planes, rows, cols), BF16),
            pltpu.VMEM((planes, rows, cols), BF16),
            pltpu.VMEM((rows, cols), F32),
            pltpu.VMEM((2, wide, hidden), F32),
            pltpu.VMEM((2, wide, hidden), F32),
            pltpu.VMEM((2, hidden, wide), F32),
            pltpu.VMEM((span, hidden), F32),
            pltpu.VMEM((span, hidden), F32),
            pltpu.VMEM((hidden, span), F32),
            pltpu.VMEM((width, 2, take, hidden), BF16),
            pltpu.VMEM((width, hidden, take), BF16),
            pltpu.VMEM((width, 2, take, hidden), BF16),
            pltpu.VMEM((width, hidden, take), BF16),
            pltpu.VMEM((rows, model), BF16),
            pltpu.VMEM((rows, cols), BF16),
            pltpu.VMEM((planes, 1, slots), F32),
            pltpu.VMEM((planes, 1, slots), F32),
            pltpu.VMEM((planes, 1, slots), F32),
            pltpu.VMEM((8, model), F32),
            pltpu.VMEM((8, model), F32),
            pltpu.VMEM((1, hidden), F32),
            dma((8,)),
            dma((2, far)),
            dma((2, 2, planes, 2)),
            dma((2, planes, 2)),
            dma((2, planes, width, 2)),
            dma((2, planes, width, 2)),
            dma((2, planes)),
            dma((2, planes, width)),
            dma((2, planes)),
            dma((2, width, 2)),
            dma((2, 3)),
            dma((2, experts)),
            dma((2, experts)),
            dma((2, 3)),
        ],
        compiler_params=pltpu.CompilerParams(has_side_effects=True, vmem_limit_bytes=67043328),
        name="layer",
    )(table, tokens, cotangent, w_gate, w_up, w_down, sh_gate, sh_up, sh_down)


def local(planes, tokens, expert_ids, gates, cotangent, w_gate, w_up, w_down, sh_gate, sh_up, sh_down):
    experts = lax.axis_size("ep")
    width = experts // planes
    q = lax.axis_index("ep") % width
    rows, model = tokens.shape
    top_count = expert_ids.shape[1]
    capacity = 3 * rows * top_count // (2 * experts)

    lanes = jnp.arange(experts, dtype=jnp.int32)
    earlier = jnp.tril(jnp.ones((rows, rows), BF16), -1)
    mine = expert_ids[:, :, None] == lanes
    names = jnp.any(mine, axis=1)
    rank = jnp.dot(earlier, names.astype(BF16), preferred_element_type=F32)
    rank = jnp.where(names, rank.astype(jnp.int32), -1)
    gate_of = jnp.sum(jnp.where(mine, gates[:, :, None], 0.0), axis=1)
    table = jnp.stack([rank.T.astype(F32), gate_of.T]).reshape(2, planes, width, 1, rows)
    cap = -(-capacity // 8) * 8
    (token_grad, grad_g, grad_u, grad_d, out_g, out_u, out_d, norms, down, shared_down, gate_rows) = layer(
        planes, cap, table, tokens, cotangent, w_gate[0], w_up[0], w_down[0], sh_gate, sh_up, sh_down
    )
    back_gate = lax.dynamic_slice_in_dim(gate_rows.reshape(experts, width, cap), q, 1, 1)[:, 0]
    slots = jnp.arange(cap, dtype=jnp.int32)
    picked = rank.T[:, None, :] == slots[None, :, None]
    token_gate = jnp.sum(jnp.where(picked, back_gate[:, :, None], 0.0), axis=1)
    gate_grad = jnp.sum(jnp.where(mine, token_gate.T[:, None, :], 0.0), axis=2) / gates
    take = model // experts
    return (
        token_grad,
        gate_grad,
        grad_g[None],
        grad_u[None],
        grad_d[None],
        out_g,
        out_u,
        out_d,
        norms[0:1],
        norms[1:2],
        down,
        norms[2, :take],
        norms[3, :take],
        jnp.sum(shared_down[:, 0], axis=0),
    )


def solution(mesh):
    placed = (
        P("ep", None),
        P("ep", None),
        P("ep", None),
        P("ep", None),
        P("ep", None, "tp"),
        P("ep", None, "tp"),
        P("ep", "tp", None),
        P(None, "tp"),
        P(None, "tp"),
        P("tp", None),
    )
    return jax.shard_map(
        functools.partial(local, plane_count(mesh)),
        mesh=mesh,
        in_specs=placed,
        out_specs=(
            P("ep", "tp"),
            P("ep", None),
            P("ep", None, "tp"),
            P("ep", None, "tp"),
            P("ep", "tp", None),
            P("ep", "tp"),
            P("ep", "tp"),
            P("tp", "ep"),
            P("ep", None),
            P("ep", None),
            P("ep", "tp"),
            P("ep"),
            P("ep"),
            P("tp"),
        ),
        check_vma=False,
    )
```

time: 257 us -> 181 us (0.70)
  the two profiles are of different devices: /device:TPU:0 before, /device:TPU:16 now
where the time goes in v1:
time: 181 us; the launch traced here: 180 us
  Pallas kernels  157 us (87%)
  local copies, waits for them, and re-layouts  14.2 us (8%)
  other arithmetic  7.21 us (4%)
    pallas_call x1, Pallas kernels, layer(): pl.pallas_call(functools.partial(layer_kernel, planes, width, cap), out_s...  157 us
    unnamed x20, local copies, waits for them, and re-layouts  11.3 us

profile of v1, /device:TPU:16, one launch (start us, length us, event | category | flops | bytes accessed | tf_op | source)
XLA Modules:
  0.0 179.9 jit_solution(1577835791794584420)
XLA Ops:
  0.7 0.7 fusion.6
  1.4 0.7 select_reduce_fusion.2
  2.1 0.9 fusion.10
  3.0 0.6 pad_maximum_fusion.table
  3.7 156.9 %layer.1 = (bf16[256,1024]{1,0:T(8,128)(2,1)}, f32[2048,256]{1,0:T(8,128)}, f32[2048,256]{1,0:T(8,128)}, f32[256,2048]{1,0:T(8,128)}, f32[128,256]{1,0:T(8,128)}...) custom-call(f32[2,4,4,1,256]{4,3,2,1,0:T(1,128)} %pad_maximum_fusion, ...), custom_call_target="tpu_custom_call" | custom-call | tf_op jit(solution)/shard_map/layer/pallas_call | solution.py:573
  160.5 1.3 reduce_sum.39
  161.8 1.3 slice_bitcast_fusion
  163.1 1.5 fusion.9
  164.6 0.8 reduce.1
  165.4 0.1 reshape.41
  165.5 1.0 select_reduce_fusion
  166.6 0.7 select_reduce_fusion.1
  167.3 1.3 div.3
  168.6 1.9 %copy.34 = bf16[256,1024]{1,0:T(8,128)(2,1)} copy(bf16[256,1024]{1,0:T(8,128)(2,1)} %get-tuple-element.56) | data formatting | bytes 1048576
  170.5 0.0 copy-start.1
  170.5 3.2 %copy.35 = f32[1,2048,256]{2,1,0:T(8,128)} copy(f32[1,2048,256]{2,1,0:T(8,128)} %bitcast.18) | data formatting | bytes 4194304
  173.7 0.0 copy-done.1
  173.7 0.0 copy-start
  173.7 1.3 copy.36
  175.0 1.0 copy-done
  176.0 0.0 copy-start.4
  176.0 0.0 copy-start.3
  176.0 0.0 copy-start.2
  176.0 0.0 copy-start.5
  176.0 1.3 copy.37
  177.3 0.0 copy-done.4
  177.3 0.7 copy.38
  178.0 0.0 copy-done.3
  178.0 0.7 copy.39
  178.7 0.0 copy-done.2
  178.7 0.7 copy.40
  179.3 0.0 copy-done.5
  179.3 0.6 copy.41
  (4 shorter events, 0.1 us)
Async XLA Ops:
  170.5 3.2 %copy-start.1 = (f32[2048,256]{1,0:T(8,128)S(1)}, f32[2048,256]{1,0:T(8,128)}, u32[]{:S(2)}) copy-start(f32[2048,256]{1,0:T(8,128)} %get-tuple-element.28) | copy-start | bytes 6291460
  173.7 2.3 %copy-start = (f32[256,2048]{1,0:T(8,128)S(1)}, f32[256,2048]{1,0:T(8,128)}, u32[]{:S(2)}) copy-start(f32[256,2048]{1,0:T(8,128)} %get-tuple-element.29) | copy-start | bytes 6291460
  176.0 1.3 copy-start.4
  176.0 2.0 %copy-start.3 = (f32[128,256]{1,0:T(8,128)S(1)}, f32[128,256]{1,0:T(8,128)}, u32[]{:S(2)}) copy-start(f32[128,256]{1,0:T(8,128)} %get-tuple-element.62) | copy-start | bytes 393220
  176.0 2.6 %copy-start.2 = (f32[256,128]{1,0:T(8,128)S(1)}, f32[256,128]{1,0:T(8,128)}, u32[]{:S(2)}) copy-start(f32[256,128]{1,0:T(8,128)} %get-tuple-element.63) | copy-start | bytes 393220
  176.0 3.3 %copy-start.5 = (f32[1,256]{1,0:T(1,128)S(1)}, f32[1,256]{1,0:T(1,128)}, u32[]{:S(2)}) copy-start(f32[1,256]{1,0:T(1,128)} %get-tuple-element.66) | copy-start | bytes 3076

commit v2 on v1

--- a/solution.py
+++ b/solution.py
@@ -63,16 +63,18 @@
 
 def layer_kernel(
     planes, width, cap,
-    table, tokens, cotangent, wg_in, wu_in, wd_in, sg_in, su_in, sd_in,
-    tok_out, gg_out, gu_out, gd_out, sg_out, su_out, sd_out, norm_out, down_out, sdn_out, gate_out,
-    toks, cots, line_table, ready, land_t, land_c,
+    ids, gates, tokens, cotangent, wg_in, wu_in, wd_in, sg_in, su_in, sd_in,
+    tok_out, gate_out, gg_out, gu_out, gd_out, sg_out, su_out, sd_out,
+    gn_out, un_out, dn_out, sgn_out, sun_out, sdn_out,
+    toks, cots, own_table, line_table, ready, land_t, land_c,
     w_g, w_u, w_d, s_g, s_u, s_d,
-    hid, dgate, dup, tp_in, ret_in, z_out, z_in, routed,
+    hid, dgate, dup, act, slant, tp_in, ret_in, z_out, z_in, routed,
     stage_g, stage_u, stage_d, acc_g, acc_u, acc_d,
     deal_gu, deal_d, deal_gu_in, deal_d_in, sh_part, sh_in,
-    gate_part, gate_in, gate_sum, norm_part, norm_in, sdn_part,
+    gate_part, gate_in, gate_sum, gate_back, norm_part, norm_in, sdn_part, sdn_in,
+    tok_done, gate_done, sg_done, su_done, sd_done, gn_done, un_done, dn_done, sgn_done, sun_done, sdn_done,
     load_sem, table_sem, line_sem, share_sem, plane_sem, pair_sem, tp_sem, ret_sem, z_sem,
-    deal_sem, misc_sem, gate_sem, sdn_sem, stage_sem,
+    deal_sem, misc_sem, pair_gate_sem, gate_sem, sdn_sem, stage_sem, out_sem,
 ):
     me, core = lax.axis_index("ep"), lax.axis_index("tp")
     z, q = me // width, me % width
@@ -109,30 +111,77 @@
             )
         )
     ]
-    for load in loads:
+    for load in loads[:2]:
         load.start()
-
-    def table_copy(step):
-        peer = (z + step) % planes * width + q
-        return copy_to(
-            table, line_table.at[z], table_sem.at[0, step - 1], table_sem.at[1, step - 1], peer, core
-        )
-
-    for step in range(1, planes):
-        table_copy(step).start()
-    line_table[z] = table[...]
-
-    def line_copy(way, block, part):
+    flushed = []
+    barrier = pltpu.get_barrier_semaphore()
+
+    def greet(ep, tp):
+        pl.semaphore_signal(
+            barrier, inc=1, device_id=(ep, tp), device_id_type=pl.DeviceIdType.MESH
+        )
+
+    def greet_peer(step, carry):
+        greet((me + step) % experts, core)
+        return carry
+
+    greet(me, 1 - core)
+    lax.fori_loop(1, experts, greet_peer, 0)
+
+    def flush(src, dst):
+        copy = pltpu.make_async_copy(src, dst, out_sem.at[len(flushed)])
+        copy.start()
+        flushed.append(copy)
+
+    def onward(way):
+        there = z + 1 - 2 * way
+        return (there >= 0) & (there < planes)
+
+    def line_copy(way, block, part, source=None):
         there = jnp.clip(z + 1 - 2 * way, 0, planes - 1)
         ref = parts[part].at[block, :, mine]
         return copy_to(
-            ref, ref, line_sem.at[0, way, block, part], line_sem.at[1, way, block, part],
+            ref if source is None else source,
+            ref,
+            line_sem.at[0, way, block, part],
+            line_sem.at[1, way, block, part],
+            there * width + q,
+            core,
+        )
+
+    def line_start(part, source):
+        for way in range(2):
+
+            @pl.when(onward(way))
+            def _():
+                line_copy(way, z, part, source.at[:, mine]).start()
+
+    named = lax.broadcasted_iota(jnp.int32, (experts, rows), 0)
+    names, gate_of = jnp.zeros((experts, rows), F32), jnp.zeros((experts, rows), F32)
+    for k in range(ids.shape[0]):
+        same = named == ids[k : k + 1, :]
+        names = names + jnp.where(same, 1.0, 0.0)
+        gate_of = gate_of + jnp.where(same, gates[k : k + 1, :], 0.0)
+    before = lax.broadcasted_iota(jnp.int32, (rows, rows), 0) < lax.broadcasted_iota(jnp.int32, (rows, rows), 1)
+    rank = dot(names.astype(BF16), jnp.where(before, 1.0, 0.0).astype(BF16))
+    rank = jnp.where(names > 0.0, rank, -1.0)
+    for e in range(experts):
+        own_table[e // width, 0, e % width] = rank[e : e + 1, :]
+        own_table[e // width, 1, e % width] = gate_of[e : e + 1, :]
+    line_table[z] = own_table[z]
+    pl.semaphore_wait(barrier, experts)
+    line_start(0, tokens)
+
+    def table_copy(step):
+        there = (z + step) % planes
+        return copy_to(
+            own_table.at[there], line_table.at[z], table_sem.at[0, step - 1], table_sem.at[1, step - 1],
             there * width + q, core,
         )
 
-    def onward(way):
-        there = z + 1 - 2 * way
-        return (there >= 0) & (there < planes)
+    for step in range(1, planes):
+        table_copy(step).start()
+    line_start(1, cotangent)
 
     def share_copy(block, part):
         ref = parts[part].at[block, :, mine]
@@ -174,14 +223,17 @@
         )
 
     def hits(block):
-        ranks = line_table[block, 0, z]
+        ranks = line_table[block, 0]
         at = lax.broadcasted_iota(jnp.int32, (width, cap, rows), 1).astype(F32)
         return (at == ranks).reshape(slots, rows)
 
-    def each(step, act):
-        def one(way, carry):
+    inner = jnp.where(2 * z <= planes - 1, 1, 0)
+
+    def each(step, act, ranks=(0, 2)):
+        def one(rank, carry):
+            way = inner + rank - 2 * inner * rank
             block = z - step + 2 * step * way
-            valid = (step >= 0) & (block >= 0) & (block < planes) & ((step > 0) | (way == 0))
+            valid = (step >= 0) & (block >= 0) & (block < planes) & ((step > 0) | (rank == 0))
 
             @pl.when(valid)
             def _():
@@ -189,15 +241,14 @@
 
             return carry
 
-        lax.fori_loop(0, 2, one, 0)
+        lax.fori_loop(*ranks, one, 0)
 
     def select(part, block):
         hit = hits(block)
         picked = dot(jnp.where(hit, 1.0, 0.0).astype(BF16), parts[part][block, :, mine])
         if part == 1:
-            gates = line_table[block, 1, z]
-            gates = jnp.broadcast_to(gates, (width, cap, rows)).reshape(slots, rows)
-            picked = picked * jnp.sum(jnp.where(hit, gates, 0.0), axis=1, keepdims=True)
+            gate_of = jnp.broadcast_to(line_table[block, 1], (width, cap, rows)).reshape(slots, rows)
+            picked = picked * jnp.sum(jnp.where(hit, gate_of, 0.0), axis=1, keepdims=True)
         ready[block, part] = picked.astype(BF16).reshape(width, cap, cols)
 
         def one(d, carry):
@@ -208,15 +259,26 @@
         lands[part][block, q, :, mine] = ready[block, part, q]
         pair_copy(block, 0, part).start()
 
-    def pass_on(block, way):
-        for part in range(2):
-
-            def one(d, carry):
-                landed(lands[part].at[block, q, :, mine], plane_sem.at[1, block, d, part])
-                pair_copy(block, d, part).start()
-                return carry
-
-            lax.fori_loop(1, width, one, 0)
+    def pass_on(part, block):
+        def one(d, carry):
+            landed(lands[part].at[block, q, :, mine], plane_sem.at[1, block, d, part])
+            pair_copy(block, d, part).start()
+            return carry
+
+        lax.fori_loop(1, width, one, 0)
+
+    def paired(part, block):
+        def one(d, carry):
+            landed(lands[part].at[block, (q + width - d) % width, :, other], pair_sem.at[1, block, d, part])
+            return carry
+
+        lax.fori_loop(0, width, one, 0)
+
+        def freed(d, carry):
+            sent(ready.at[block, part, 0], plane_sem.at[0, block, d, part])
+            return carry
+
+        lax.fori_loop(1, width, freed, 0)
 
     def shared(block, way):
         for part in range(2):
@@ -251,32 +313,30 @@
 
     sh_copy = copy_to(sh_part.at[:, other], sh_in, misc_sem.at[0, 0], misc_sem.at[1, 0], me, 1 - core)
 
-    def compute(block, way):
-        for part in range(2):
-
-            def one(d, carry):
-                ref = lands[part].at[block, (q + width - d) % width, :, other]
-                landed(ref, pair_sem.at[1, block, d, part])
-                return carry
-
-            lax.fori_loop(0, width, one, 0)
-
-            def freed(d, carry):
-                sent(ready.at[block, part, 0], plane_sem.at[0, block, d, part])
-                return carry
-
-            lax.fori_loop(1, width, freed, 0)
+    def compute(last, block):
+        paired(0, block)
         inputs = land_t[block].reshape(slots, model)
         gate_pre = dot(inputs, w_g[...])
         up_pre = dot(inputs, w_u[...])
         active, slope = silu_parts(gate_pre)
-        h = (active * up_pre).astype(BF16)
+        act[...] = active
+        slant[...] = up_pre * slope
+        hid[block] = (active * up_pre).astype(BF16)
+
+        @pl.when(last)
+        def _():
+            pass_on(1, block)
+
+        paired(1, block)
         h_cot = dot_last(land_c[block].reshape(slots, model), w_d[...])
-        d_gate = (h_cot * up_pre * slope).astype(BF16)
-        d_up = (h_cot * active).astype(BF16)
-        hid[block] = h
+        d_gate = (h_cot * slant[...]).astype(BF16)
+        d_up = (h_cot * act[...]).astype(BF16)
         dgate[block] = d_gate
         dup[block] = d_up
+        gate_row = row_sums(hid[block].astype(F32) * h_cot)
+        for w in range(width):
+            gate_part[block, w, :, :cap] = gate_row[:, w * cap : (w + 1) * cap]
+        gate_pair(block).start()
         wide = cols // 2
 
         def half(which):
@@ -299,7 +359,36 @@
             return carry
 
         lax.fori_loop(0, 2, one, 0)
-        gate_part[block] = row_sums(h.astype(F32) * h_cot)
+
+    def gate_pair(block):
+        return copy_to(
+            gate_part.at[block], gate_in.at[block], pair_gate_sem.at[0, block], pair_gate_sem.at[1, block],
+            me, 1 - core,
+        )
+
+    def gate_copy(block, d):
+        to_q = (q + d) % width
+        return copy_to(
+            gate_sum.at[block, to_q], gate_back.at[me], gate_sem.at[0, block, d], gate_sem.at[1, z, d],
+            block * width + to_q, core,
+        )
+
+    def gate_sends(block, way):
+        gate_pair(block).wait_recv()
+        gate_sum[block] = gate_part[block] + gate_in[block]
+
+        def one(d, carry):
+            @pl.when((block != z) | (d > 0))
+            def _():
+                gate_copy(block, d).start()
+
+            return carry
+
+        lax.fori_loop(0, width, one, 0)
+
+        @pl.when(block == z)
+        def _():
+            gate_back[me] = gate_sum[z, q]
 
     def sums(block, way):
         landed(tp_in.at[block], tp_sem.at[1, block])
@@ -330,17 +419,14 @@
             z_out[block] = back.astype(BF16)
             z_copy(block).start()
 
-    for part in range(2):
-        loads[part].wait()
-        for way in range(2):
-
-            @pl.when(onward(way))
-            def _():
-                line_copy(way, z, part).start()
-
+    for load in loads[:2]:
+        load.wait()
+    for load in loads[2:]:
+        load.start()
     acc_g[...] = jnp.zeros_like(acc_g)
     acc_u[...] = jnp.zeros_like(acc_u)
     acc_d[...] = jnp.zeros_like(acc_d)
+    gate_part[...] = jnp.zeros_like(gate_part)
 
     def body(step, carry):
         @pl.when(step == 1)
@@ -350,6 +436,26 @@
             for other_step in range(1, planes):
                 landed(line_table.at[z], table_sem.at[1, other_step - 1])
 
+        def expert(last, block):
+            compute(last, block)
+
+            @pl.when(block != z)
+            def _():
+                sums(block, 0)
+
+            gate_sends(block, 0)
+
+        def ahead(block, way):
+            pass_on(0, block)
+            pass_on(1, block)
+            expert(False, block)
+
+        early = (step == 2) & between
+
+        @pl.when(early)
+        def _():
+            each(1, ahead, (0, 1))
+
         for part in range(2):
 
             def arrive(block, way):
@@ -364,14 +470,39 @@
                     share_copy(block, part).start()
 
             each(step, arrive)
-            each(step, lambda block, way: select(part, block))
+            each(step, lambda block, way: select(part, block), (0, 1))
+
+        def select_both(block, way):
+            for part in range(2):
+                select(part, block)
+
+        each(step, select_both, (1, 2))
+        last = step == planes
+        start = jnp.where(early, 1, 0)
+
+        @pl.when((step > 2) & (step < planes))
+        def _():
+            each(step - 2, scatter, (0, 1))
+
+        def hand_on(block, way):
+            pass_on(0, block)
+
+            @pl.when(jnp.logical_not(last))
+            def _():
+                pass_on(1, block)
+
+        each(step - 1, hand_on, (start, 2))
         each(step - 1, shared)
-        each(step - 1, pass_on)
-        each(step - 1, compute)
-        each(step - 1, sums)
-        each(step - 2, scatter)
+
+        each(step - 1, lambda block, way: expert(last, block), (start, 2))
+
+        @pl.when(step > 2)
+        def _():
+            each(step - 2, scatter, (jnp.where(last, 0, 1), 2))
+
         return carry
 
+    between = (z > 0) & (z < planes - 1)
     lax.fori_loop(0, planes + 1, body, 0)
 
     for p in range(width):
@@ -394,24 +525,7 @@
         return carry
 
     lax.fori_loop(1, width, deal, 0)
-    gate_pair = copy_to(gate_part, gate_in, misc_sem.at[0, 1], misc_sem.at[1, 1], me, 1 - core)
-    gate_pair.start()
-    gate_pair.wait_recv()
-    gate_sum[...] = gate_part[...] + gate_in[...]
-    gate_out[me] = gate_sum[z]
-
-    def gate_copy(step):
-        peer = (me + step) % experts
-        return copy_to(
-            gate_sum.at[peer // width], gate_out.at[me], gate_sem.at[0, step], gate_sem.at[1, step], peer, core
-        )
-
-    def send_gate(step, carry):
-        gate_copy(step).start()
-        return carry
-
-    lax.fori_loop(1, experts, send_gate, 0)
-
+    sums(z, 0)
     wide = stage_g.shape[1]
     chunks = model // wide
 
@@ -423,7 +537,7 @@
             pltpu.make_async_copy(stage_d.at[slot], gd_out.at[:, at], stage_sem.at[slot, 2]),
         )
 
-    down_out[...] = jnp.zeros_like(down_out)
+    dn_done[...] = jnp.zeros_like(dn_done)
     norm_part[...] = jnp.zeros_like(norm_part)
 
     def weight_grads(i, carry):
@@ -445,13 +559,18 @@
         block_rows = land_c[:, :, :, at].reshape(planes * slots, wide)
         grad = dot_first(hid[...].reshape(planes * slots, hidden), block_rows)
         stage_d[slot] = grad
-        down_out[...] += row_sums(grad * grad)
+        dn_done[...] += row_sums(grad * grad)
         for copy in stage_copies(i, slot):
             copy.start()
+
+        @pl.when(i == chunks // 4)
+        def _():
+            each(planes - 1, scatter)
+
         return carry
 
     lax.fori_loop(0, chunks, weight_grads, 0)
-    each(planes - 1, scatter)
+    flush(dn_done, dn_out)
 
     def deal_done(d, carry):
         for copy in deal_copies(d):
@@ -464,19 +583,22 @@
         grad_g = grad_g + deal_gu_in[d, 0].astype(F32)
         grad_u = grad_u + deal_gu_in[d, 1].astype(F32)
         grad_d = grad_d + deal_d_in[d].astype(F32)
-    sg_out[...] = grad_g
-    su_out[...] = grad_u
-    sd_out[...] = grad_d
+    sg_done[...] = grad_g
+    su_done[...] = grad_u
+    sd_done[...] = grad_d
+    flush(sg_done, sg_out)
+    flush(su_done, su_out)
+    flush(sd_done, sd_out)
     norm_part[2:3, :take] = row_sums(grad_g * grad_g)
     norm_part[3:4, :take] = row_sums(grad_u * grad_u)
     norm_pair = copy_to(norm_part, norm_in, misc_sem.at[0, 2], misc_sem.at[1, 2], me, 1 - core)
     norm_pair.start()
     sdn_part[...] = row_sums(grad_d * grad_d)
-    sdn_out[me] = sdn_part[...]
+    sdn_in[me] = sdn_part[...]
 
     def sdn_copy(step):
         return copy_to(
-            sdn_part, sdn_out.at[me], sdn_sem.at[0, step], sdn_sem.at[1, step], (me + step) % experts, core
+            sdn_part, sdn_in.at[me], sdn_sem.at[0, step], sdn_sem.at[1, step], (me + step) % experts, core
         )
 
     def send_sdn(step, carry):
@@ -484,11 +606,46 @@
         return carry
 
     lax.fori_loop(1, experts, send_sdn, 0)
+    norm_pair.wait_recv()
+    total = norm_part[...] + norm_in[...]
+    gn_done[...] = total[0:1]
+    un_done[...] = total[1:2]
+    sgn_done[...] = total[2:3, :take]
+    sun_done[...] = total[3:4, :take]
+    flush(gn_done, gn_out)
+    flush(un_done, un_out)
+    flush(sgn_done, sgn_out)
+    flush(sun_done, sun_out)
+
+    def gate_arrived(source, carry):
+        def one(d, inner):
+            @pl.when((source != z) | (d > 0))
+            def _():
+                landed(gate_back.at[me], gate_sem.at[1, source, d])
+
+            return inner
+
+        return lax.fori_loop(0, width, one, carry)
+
+    lax.fori_loop(0, planes, gate_arrived, 0)
+    top, lanes = ids.shape[0], gate_back.shape[2]
+
+    def gate_rows(e, total):
+        at = lax.broadcasted_iota(jnp.int32, (lanes, rows), 0).astype(F32)
+        hit = jnp.where(at == own_table[e // width, 0, e % width], 1.0, 0.0)
+        back = lax.dot_general(
+            jnp.broadcast_to(gate_back[e], (8, lanes)), hit, (((1,), (0,)), ((), ())),
+            precision=lax.Precision.HIGHEST, preferred_element_type=F32,
+        )
+        return total + jnp.where(ids[...] == e, jnp.broadcast_to(back[:1], (top, rows)), 0.0)
+
+    total = lax.fori_loop(0, experts, gate_rows, jnp.zeros((top, rows), F32))
+    gate_done[...] = total / gates[...]
+    flush(gate_done, gate_out)
+
+    scatter(z, 0)
     sh_copy.wait_recv()
-    total = routed[...] + (sh_part[:, mine].astype(F32) + sh_in[...].astype(F32))
-    routed[...] = total
-    norm_pair.wait_recv()
-    norm_out[...] = norm_part[...] + norm_in[...]
+    routed[...] += sh_part[:, mine].astype(F32) + sh_in[...].astype(F32)
 
     def gather(step, carry):
         source = (z + step) % planes
@@ -497,21 +654,22 @@
         return carry
 
     lax.fori_loop(1, planes, gather, 0)
-    tok_out[...] = routed[...].astype(BF16)
+    tok_done[...] = routed[...].astype(BF16)
+    flush(tok_done, tok_out)
 
     def small_done(step, carry):
-        gate_copy(step).wait()
         sdn_copy(step).wait()
         return carry
 
     lax.fori_loop(1, experts, small_done, 0)
+    sdn_done[...] = jnp.sum(sdn_in[...], axis=0)
+    flush(sdn_done, sdn_out)
     for i in range(max(chunks - 2, 0), chunks):
         for copy in stage_copies(i, i % 2):
             copy.wait()
     for step in range(1, planes):
         table_copy(step).wait_send()
     sh_copy.wait_send()
-    gate_pair.wait_send()
     norm_pair.wait_send()
 
     def deal_sent(d, carry):
@@ -528,7 +686,7 @@
 
                 @pl.when(behind & onward(way))
                 def _():
-                    line_copy(way, block, part).wait_send()
+                    sent(parts[part].at[block, :, mine], line_sem.at[0, way, block, part])
 
             @pl.when(block != z)
             def _():
@@ -540,6 +698,16 @@
 
             lax.fori_loop(0, width, pairs, 0)
         tp_copy(block).wait_send()
+        gate_pair(block).wait_send()
+
+        def gate_sent(d, inner):
+            @pl.when((block != z) | (d > 0))
+            def _():
+                gate_copy(block, d).wait_send()
+
+            return inner
+
+        lax.fori_loop(0, width, gate_sent, 0)
 
         def returns(d, inner):
             ret_copy(block, d).wait_send()
@@ -554,12 +722,55 @@
         return carry
 
     lax.fori_loop(0, planes, drain, 0)
-
-
-def layer(planes, cap, table, tokens, cotangent, w_gate, w_up, w_down, sh_gate, sh_up, sh_down):
-    width = table.shape[2]
-    experts = planes * width
+    for copy in flushed:
+        copy.wait()
+
+
+def finish_kernel(count, *refs):
+    sources, results, held = refs[:count], refs[count : 2 * count], refs[2 * count : 3 * count]
+    in_sem, out_sem = refs[3 * count :]
+    moves = []
+    for i in range(count):
+        rows = sources[i].shape[0]
+        pieces = 4 if rows % 32 == 0 and sources[i].shape[1] * rows >= 2**18 else 1
+        step = rows // pieces
+        for p in range(pieces):
+            at = slice(p * step, (p + 1) * step)
+            moves.append(
+                (
+                    pltpu.make_async_copy(sources[i].at[at], held[i].at[at], in_sem.at[i, p]),
+                    pltpu.make_async_copy(held[i].at[at], results[i].at[at], out_sem.at[i, p]),
+                )
+            )
+    for taken, _ in moves:
+        taken.start()
+    for taken, given in moves:
+        taken.wait()
+        given.start()
+    for _, given in moves:
+        given.wait()
+
+
+def finish(arrays):
+    count = len(arrays)
+    hbm = pl.BlockSpec(memory_space=pltpu.HBM)
+    return pl.pallas_call(
+        functools.partial(finish_kernel, count),
+        out_shape=[jax.ShapeDtypeStruct(a.shape, a.dtype) for a in arrays],
+        in_specs=[hbm] * count,
+        out_specs=[hbm] * count,
+        scratch_shapes=[pltpu.VMEM(a.shape, a.dtype) for a in arrays]
+        + [pltpu.SemaphoreType.DMA((count, 4)), pltpu.SemaphoreType.DMA((count, 4))],
+        compiler_params=pltpu.CompilerParams(vmem_limit_bytes=67043328),
+        name="finish",
+    )(*arrays)
+
+
+def layer(planes, cap, ids, gates, tokens, cotangent, w_gate, w_up, w_down, sh_gate, sh_up, sh_down):
+    experts = lax.axis_size("ep")
+    width = experts // planes
     rows, model = tokens.shape
+    lanes = -(-cap // 128) * 128
     cols, hidden = model // 2, w_gate.shape[1]
     take = model // experts
     span = width * take
@@ -574,23 +785,27 @@
         functools.partial(layer_kernel, planes, width, cap),
         out_shape=(
             out((rows, cols), BF16),
+            out(gates.shape, F32),
             out((model, hidden), F32),
             out((model, hidden), F32),
             out((hidden, model), F32),
             out((take, hidden), F32),
             out((take, hidden), F32),
             out((hidden, take), F32),
-            out((8, model), F32),
+            out((1, model), F32),
+            out((1, model), F32),
             out((1, hidden), F32),
-            out((experts, 1, hidden), F32),
-            out((experts, 1, slots), F32),
+            out((1, take), F32),
+            out((1, take), F32),
+            out((1, hidden), F32),
         ),
-        in_specs=[vmem] + [hbm] * 8,
-        out_specs=(vmem, hbm, hbm, hbm) + (vmem,) * 7,
+        in_specs=[vmem] * 2 + [hbm] * 8,
+        out_specs=(hbm,) * 14,
         scratch_shapes=[
             pltpu.VMEM((planes, rows, model), BF16),
             pltpu.VMEM((planes, rows, model), BF16),
-            pltpu.VMEM((planes,) + table.shape, F32),
+            pltpu.VMEM((planes, 2, width, 1, rows), F32),
+            pltpu.VMEM((planes, 2, width, 1, rows), F32),
             pltpu.VMEM((planes, 2, width, cap, cols), BF16),
             pltpu.VMEM((planes, width, cap, model), BF16),
             pltpu.VMEM((planes, width, cap, model), BF16),
@@ -603,6 +818,8 @@
             pltpu.VMEM((planes, slots, hidden), BF16),
             pltpu.VMEM((planes, slots, hidden), BF16),
             pltpu.VMEM((planes, slots, hidden), BF16),
+            pltpu.VMEM((slots, hidden), F32),
+            pltpu.VMEM((slots, hidden), F32),
             pltpu.VMEM((planes, width, cap, cols), BF16),
             pltpu.VMEM((planes, width, cap, cols), BF16),
             pltpu.VMEM((planes, rows, cols), BF16),
@@ -620,11 +837,24 @@
             pltpu.VMEM((width, hidden, take), BF16),
             pltpu.VMEM((rows, model), BF16),
             pltpu.VMEM((rows, cols), BF16),
-            pltpu.VMEM((planes, 1, slots), F32),
-            pltpu.VMEM((planes, 1, slots), F32),
-            pltpu.VMEM((planes, 1, slots), F32),
+            pltpu.VMEM((planes, width, 1, lanes), F32),
+            pltpu.VMEM((planes, width, 1, lanes), F32),
+            pltpu.VMEM((planes, width, 1, lanes), F32),
+            pltpu.VMEM((experts, 1, lanes), F32),
             pltpu.VMEM((8, model), F32),
             pltpu.VMEM((8, model), F32),
+            pltpu.VMEM((1, hidden), F32),
+            pltpu.VMEM((experts, 1, hidden), F32),
+            pltpu.VMEM((rows, cols), BF16),
+            pltpu.VMEM(gates.shape, F32),
+            pltpu.VMEM((take, hidden), F32),
+            pltpu.VMEM((take, hidden), F32),
+            pltpu.VMEM((hidden, take), F32),
+            pltpu.VMEM((1, model), F32),
+            pltpu.VMEM((1, model), F32),
+            pltpu.VMEM((1, hidden), F32),
+            pltpu.VMEM((1, take), F32),
+            pltpu.VMEM((1, take), F32),
             pltpu.VMEM((1, hidden), F32),
             dma((8,)),
             dma((2, far)),
@@ -637,56 +867,43 @@
             dma((2, planes)),
             dma((2, width, 2)),
             dma((2, 3)),
-            dma((2, experts)),
+            dma((2, planes)),
+            dma((2, planes, width)),
             dma((2, experts)),
             dma((2, 3)),
+            dma((16,)),
         ],
-        compiler_params=pltpu.CompilerParams(has_side_effects=True, vmem_limit_bytes=67043328),
+        compiler_params=pltpu.CompilerParams(collective_id=0, has_side_effects=True, vmem_limit_bytes=67043328),
         name="layer",
-    )(table, tokens, cotangent, w_gate, w_up, w_down, sh_gate, sh_up, sh_down)
+    )(ids, gates, tokens, cotangent, w_gate, w_up, w_down, sh_gate, sh_up, sh_down)
 
 
 def local(planes, tokens, expert_ids, gates, cotangent, w_gate, w_up, w_down, sh_gate, sh_up, sh_down):
     experts = lax.axis_size("ep")
-    width = experts // planes
-    q = lax.axis_index("ep") % width
-    rows, model = tokens.shape
-    top_count = expert_ids.shape[1]
+    rows, top_count = expert_ids.shape
     capacity = 3 * rows * top_count // (2 * experts)
-
-    lanes = jnp.arange(experts, dtype=jnp.int32)
-    earlier = jnp.tril(jnp.ones((rows, rows), BF16), -1)
-    mine = expert_ids[:, :, None] == lanes
-    names = jnp.any(mine, axis=1)
-    rank = jnp.dot(earlier, names.astype(BF16), preferred_element_type=F32)
-    rank = jnp.where(names, rank.astype(jnp.int32), -1)
-    gate_of = jnp.sum(jnp.where(mine, gates[:, :, None], 0.0), axis=1)
-    table = jnp.stack([rank.T.astype(F32), gate_of.T]).reshape(2, planes, width, 1, rows)
     cap = -(-capacity // 8) * 8
-    (token_grad, grad_g, grad_u, grad_d, out_g, out_u, out_d, norms, down, shared_down, gate_rows) = layer(
-        planes, cap, table, tokens, cotangent, w_gate[0], w_up[0], w_down[0], sh_gate, sh_up, sh_down
+    arrays = layer(
+        planes, cap, expert_ids.T, gates.T, tokens, cotangent,
+        w_gate[0], w_up[0], w_down[0], sh_gate, sh_up, sh_down,
     )
-    back_gate = lax.dynamic_slice_in_dim(gate_rows.reshape(experts, width, cap), q, 1, 1)[:, 0]
-    slots = jnp.arange(cap, dtype=jnp.int32)
-    picked = rank.T[:, None, :] == slots[None, :, None]
-    token_gate = jnp.sum(jnp.where(picked, back_gate[:, :, None], 0.0), axis=1)
-    gate_grad = jnp.sum(jnp.where(mine, token_gate.T[:, None, :], 0.0), axis=2) / gates
-    take = model // experts
+    (token_grad, gate_grad, grad_g, grad_u, grad_d, out_g, out_u, out_d, gate_norms, up_norms, down_norms,
+     shared_gate, shared_up, shared_down) = finish(arrays)
     return (
         token_grad,
-        gate_grad,
+        gate_grad.T,
         grad_g[None],
         grad_u[None],
         grad_d[None],
         out_g,
         out_u,
         out_d,
-        norms[0:1],
-        norms[1:2],
-        down,
-        norms[2, :take],
-        norms[3, :take],
-        jnp.sum(shared_down[:, 0], axis=0),
+        gate_norms,
+        up_norms,
+        down_norms,
+        shared_gate[0],
+        shared_up[0],
+        shared_down[0],
     )
 
 

time: 181 us -> 149 us (0.82)
  the two profiles are of different devices: /device:TPU:16 before, /device:TPU:0 now
where the time goes in v2:
time: 149 us; the launch traced here: 148 us
  Pallas kernels  148 us (99%)
    pallas_call x1, Pallas kernels, layer(): pl.pallas_call(functools.partial(layer_kernel, planes, width, cap), out_s...  141 us
    pallas_call x1, Pallas kernels, finish(): pl.pallas_call(functools.partial(finish_kernel, count), out_shape=[jax.Sh...  6.63 us

profile of v2, /device:TPU:0, one launch (start us, length us, event | category | flops | bytes accessed | tf_op | source)
XLA Modules:
  0.0 148.3 jit_solution(2572204825706568810)
XLA Ops:
  0.7 141.0 %layer.1 = (bf16[256,1024]{1,0:T(8,128)(2,1)}, f32[4,256]{1,0:T(4,128)}, f32[2048,256]{1,0:T(8,128)}, f32[2048,256]{1,0:T(8,128)}, f32[256,2048]{1,0:T(8,128)}, ...) custom-call(s32[4,256]{1,0:T(4,128)} %bitcast.15, ...), custom_call_target="tpu_custom_call" | custom-call | tf_op jit(solution)/shard_map/layer/pallas_call | solution.py:784
  141.7 6.6 %finish.1 = (bf16[256,1024]{1,0:T(8,128)(2,1)}, f32[4,256]{1,0:T(4,128)}, f32[2048,256]{1,0:T(8,128)}, f32[2048,256]{1,0:T(8,128)}, f32[256,2048]{1,0:T(8,128)},...) custom-call(bf16[256,1024]{1,0:T(8,128)(2,1)} %get-tuple-element.42., ...), custom_call_target="tpu_custom_call" | custom-call | tf_op jit(solution)/shard_map/finish/pallas_call | solution.py:757

commit v3 on v2

--- a/solution.py
+++ b/solution.py
@@ -451,6 +451,7 @@
             expert(False, block)
 
         early = (step == 2) & between
+        edge = (step < planes) & jnp.logical_not(between)
 
         @pl.when(early)
         def _():
@@ -471,18 +472,27 @@
 
             each(step, arrive)
             each(step, lambda block, way: select(part, block), (0, 1))
+            if part == 0:
+
+                @pl.when(edge)
+                def _():
+                    each(step - 1, ahead, (0, 1))
 
         def select_both(block, way):
             for part in range(2):
                 select(part, block)
 
         each(step, select_both, (1, 2))
-        last = step == planes
-        start = jnp.where(early, 1, 0)
-
-        @pl.when((step > 2) & (step < planes))
+        last = step > jnp.maximum(z, planes - 1 - z)
+        start = jnp.where(early | edge, 1, 0)
+
+        @pl.when(step > 2)
         def _():
             each(step - 2, scatter, (0, 1))
+
+        @pl.when((step == planes) & jnp.logical_not(between))
+        def _():
+            sums(z, 0)
 
         def hand_on(block, way):
             pass_on(0, block)
@@ -498,7 +508,7 @@
 
         @pl.when(step > 2)
         def _():
-            each(step - 2, scatter, (jnp.where(last, 0, 1), 2))
+            each(step - 2, scatter, (1, 2))
 
         return carry
 
@@ -525,7 +535,11 @@
         return carry
 
     lax.fori_loop(1, width, deal, 0)
-    sums(z, 0)
+
+    @pl.when(between)
+    def _():
+        sums(z, 0)
+
     wide = stage_g.shape[1]
     chunks = model // wide
 
@@ -539,6 +553,37 @@
 
     dn_done[...] = jnp.zeros_like(dn_done)
     norm_part[...] = jnp.zeros_like(norm_part)
+
+    def sdn_copy(step):
+        return copy_to(
+            sdn_part, sdn_in.at[me], sdn_sem.at[0, step], sdn_sem.at[1, step], (me + step) % experts, core
+        )
+
+    def deal_finish():
+        def deal_done(d, carry):
+            for copy in deal_copies(d):
+                copy.wait_recv()
+            return carry
+
+        lax.fori_loop(1, width, deal_done, 0)
+        grad_g, grad_u, grad_d = deal_gu[q, 0].astype(F32), deal_gu[q, 1].astype(F32), deal_d[q].astype(F32)
+        for d in range(1, width):
+            grad_g = grad_g + deal_gu_in[d, 0].astype(F32)
+            grad_u = grad_u + deal_gu_in[d, 1].astype(F32)
+            grad_d = grad_d + deal_d_in[d].astype(F32)
+        sg_done[...] = grad_g
+        su_done[...] = grad_u
+        sd_done[...] = grad_d
+        norm_part[2:3, :take] = row_sums(grad_g * grad_g)
+        norm_part[3:4, :take] = row_sums(grad_u * grad_u)
+        sdn_part[...] = row_sums(grad_d * grad_d)
+        sdn_in[me] = sdn_part[...]
+
+        def send_sdn(step, carry):
+            sdn_copy(step).start()
+            return carry
+
+        lax.fori_loop(1, experts, send_sdn, 0)
 
     def weight_grads(i, carry):
         slot = i % 2
@@ -563,49 +608,51 @@
         for copy in stage_copies(i, slot):
             copy.start()
 
-        @pl.when(i == chunks // 4)
+        @pl.when(i == chunks // 2)
         def _():
             each(planes - 1, scatter)
+
+        @pl.when(i == max(chunks - 2, chunks // 2))
+        def _():
+            deal_finish()
 
         return carry
 
     lax.fori_loop(0, chunks, weight_grads, 0)
     flush(dn_done, dn_out)
 
-    def deal_done(d, carry):
-        for copy in deal_copies(d):
-            copy.wait_recv()
-        return carry
-
-    lax.fori_loop(1, width, deal_done, 0)
-    grad_g, grad_u, grad_d = deal_gu[q, 0].astype(F32), deal_gu[q, 1].astype(F32), deal_d[q].astype(F32)
-    for d in range(1, width):
-        grad_g = grad_g + deal_gu_in[d, 0].astype(F32)
-        grad_u = grad_u + deal_gu_in[d, 1].astype(F32)
-        grad_d = grad_d + deal_d_in[d].astype(F32)
-    sg_done[...] = grad_g
-    su_done[...] = grad_u
-    sd_done[...] = grad_d
     flush(sg_done, sg_out)
     flush(su_done, su_out)
     flush(sd_done, sd_out)
-    norm_part[2:3, :take] = row_sums(grad_g * grad_g)
-    norm_part[3:4, :take] = row_sums(grad_u * grad_u)
     norm_pair = copy_to(norm_part, norm_in, misc_sem.at[0, 2], misc_sem.at[1, 2], me, 1 - core)
     norm_pair.start()
-    sdn_part[...] = row_sums(grad_d * grad_d)
-    sdn_in[me] = sdn_part[...]
-
-    def sdn_copy(step):
-        return copy_to(
-            sdn_part, sdn_in.at[me], sdn_sem.at[0, step], sdn_sem.at[1, step], (me + step) % experts, core
-        )
-
-    def send_sdn(step, carry):
-        sdn_copy(step).start()
-        return carry
-
-    lax.fori_loop(1, experts, send_sdn, 0)
+
+    def gate_arrived(source, carry):
+        def one(d, inner):
+            @pl.when((source != z) | (d > 0))
+            def _():
+                landed(gate_back.at[me], gate_sem.at[1, source, d])
+
+            return inner
+
+        return lax.fori_loop(0, width, one, carry)
+
+    lax.fori_loop(0, planes, gate_arrived, 0)
+    top, lanes = ids.shape[0], gate_back.shape[2]
+
+    def gate_rows(e, total):
+        at = lax.broadcasted_iota(jnp.int32, (lanes, rows), 0).astype(F32)
+        hit = jnp.where(at == own_table[e // width, 0, e % width], 1.0, 0.0)
+        back = lax.dot_general(
+            jnp.broadcast_to(gate_back[e], (8, lanes)), hit, (((1,), (0,)), ((), ())),
+            precision=lax.Precision.HIGHEST, preferred_element_type=F32,
+        )
+        return total + jnp.where(ids[...] == e, jnp.broadcast_to(back[:1], (top, rows)), 0.0)
+
+    total = lax.fori_loop(0, experts, gate_rows, jnp.zeros((top, rows), F32))
+    gate_done[...] = total / gates[...]
+    flush(gate_done, gate_out)
+
     norm_pair.wait_recv()
     total = norm_part[...] + norm_in[...]
     gn_done[...] = total[0:1]
@@ -616,32 +663,6 @@
     flush(un_done, un_out)
     flush(sgn_done, sgn_out)
     flush(sun_done, sun_out)
-
-    def gate_arrived(source, carry):
-        def one(d, inner):
-            @pl.when((source != z) | (d > 0))
-            def _():
-                landed(gate_back.at[me], gate_sem.at[1, source, d])
-
-            return inner
-
-        return lax.fori_loop(0, width, one, carry)
-
-    lax.fori_loop(0, planes, gate_arrived, 0)
-    top, lanes = ids.shape[0], gate_back.shape[2]
-
-    def gate_rows(e, total):
-        at = lax.broadcasted_iota(jnp.int32, (lanes, rows), 0).astype(F32)
-        hit = jnp.where(at == own_table[e // width, 0, e % width], 1.0, 0.0)
-        back = lax.dot_general(
-            jnp.broadcast_to(gate_back[e], (8, lanes)), hit, (((1,), (0,)), ((), ())),
-            precision=lax.Precision.HIGHEST, preferred_element_type=F32,
-        )
-        return total + jnp.where(ids[...] == e, jnp.broadcast_to(back[:1], (top, rows)), 0.0)
-
-    total = lax.fori_loop(0, experts, gate_rows, jnp.zeros((top, rows), F32))
-    gate_done[...] = total / gates[...]
-    flush(gate_done, gate_out)
 
     scatter(z, 0)
     sh_copy.wait_recv()

time: 149 us -> 142 us (0.953)
  Pallas kernels: 148 us -> 141 us
    pallas_call x1, Pallas kernels: 141 us -> 134 us  [layer(): pl.pallas_call(functools.partial(layer_kernel, planes, width, cap), out_s...]
where the time goes in v3:
time: 142 us
  Pallas kernels  141 us (99%)
    pallas_call x1, Pallas kernels, layer(): pl.pallas_call(functools.partial(layer_kernel, planes, width, cap), out_s...  134 us
    pallas_call x1, Pallas kernels, finish(): pl.pallas_call(functools.partial(finish_kernel, count), out_shape=[jax.Sh...  6.63 us

profile of v3, /device:TPU:0, one launch (start us, length us, event | category | flops | bytes accessed | tf_op | source)
XLA Modules:
  0.0 141.8 jit_solution(3313742954664925444)
XLA Ops:
  0.7 134.3 %layer.1 = (bf16[256,1024]{1,0:T(8,128)(2,1)}, f32[4,256]{1,0:T(4,128)}, f32[2048,256]{1,0:T(8,128)}, f32[2048,256]{1,0:T(8,128)}, f32[256,2048]{1,0:T(8,128)}, ...) custom-call(s32[4,256]{1,0:T(4,128)} %bitcast.15, ...), custom_call_target="tpu_custom_call" | custom-call | tf_op jit(solution)/shard_map/layer/pallas_call | solution.py:805
  135.0 6.6 %finish.1 = (bf16[256,1024]{1,0:T(8,128)(2,1)}, f32[4,256]{1,0:T(4,128)}, f32[2048,256]{1,0:T(8,128)}, f32[2048,256]{1,0:T(8,128)}, f32[256,2048]{1,0:T(8,128)},...) custom-call(bf16[256,1024]{1,0:T(8,128)(2,1)} %get-tuple-element.42., ...), custom_call_target="tpu_custom_call" | custom-call | tf_op jit(solution)/shard_map/finish/pallas_call | solution.py:778
